TPU v7x, 256 devices: a 4x2x16 block of a 4x16x16 slice. The times are simulated.
256 devices in a mesh: grp: 2 (over y), sp: 16 (over z), tp: 8 (over x, core).
Axes of the slice: x: 4, y: 2, z: 16, core: 2. Of those that a mesh axis runs over, the one named last changes fastest.
The devices are a block of a 4x16x16 slice.
Arguments:
- tokens: bfloat16 [2, 16384, 2048], P('grp', ('sp', 'tp')), parts along dimension 0, may hold values from -6 to 6
- norm_gain: bfloat16 [2048], replicated, may hold values from 0.099609375 to 1.8984375
- w_query: bfloat16 [2048, 1024], P('sp'), may hold values from -0.125 to 0.125
- w_forget: bfloat16 [2048, 1024], P('sp'), may hold values from -0.125 to 0.125
- w_input: bfloat16 [2048, 1024], P('sp'), may hold values from -0.125 to 0.125
- floor_gap: float32 [1024], replicated, may hold values from 1.8310547e-05 to 0.12
- extra_decay: float32 [2, 16384, 16], P('grp', ('sp', 'tp')), parts along dimension 0, may hold values from -1.4 to 0, as said below
- init_state: float32 [2, 16, 64, 64], P('grp'), parts along dimension 0, may hold values from -0.03125 to 0.03125
- head_norm_gain: bfloat16 [1024], replicated, may hold values from 0.099609375 to 1.8984375
- w_output: bfloat16 [1024, 2048], P(None, 'sp'), may hold values from -0.1875 to 0.1875
Outputs:
- mixed: bfloat16 [2, 16384, 2048], P('grp', ('sp', 'tp')), parts along dimension 0
- final_state: float32 [2, 65536], P('grp', ('sp', 'tp')), parts along dimension 0
There are 2 independent parts, one for each index of `grp`. A program takes and returns all parts, laid end to end along the dimension named above; an argument that names none is the same for every part. Nothing has to cross between parts.
Inputs may be any that keep to these rules, and one draw needn't show every extreme that they name: `extra_decay`: no entry is positive.
All inputs are finite; a program needn't handle non-finite values.
Results may differ from a plain program's by a relative error of at most 0.014.
Values may be sent and summed in bfloat16 or wider, within the bound.
A program may use at most 128 MiB of HBM per device.

v0:
```python
import jax
import jax.numpy as jnp
from jax import lax
from jax.sharding import Mesh
from jax.sharding import PartitionSpec as P

HEADS = 16
HEAD = 64
BLOCK = 64
SP_TP = ("sp", "tp_0", "tp_1")


EPSILON = 1e-05


def nothing_yet(value, identity):
    return jax.tree.map(
        lambda a, e: jnp.broadcast_to(jnp.asarray(e, a.dtype), a.shape), value, identity
    )


def entering_2(value, axes, combine, identity):
    before = start = nothing_yet(value, identity)
    total = value
    for axis in reversed(axes):
        peers, mine = (lax.axis_size(axis), lax.axis_index(axis))
        pieces = jax.tree.map(
            lambda part, kind: lax.all_gather(part.astype(kind), axis),
            total,
            (jnp.bfloat16, jnp.bfloat16),
        )
        inside, total = (start, start)
        for k in range(peers):
            passed = k < mine
            total = combine(
                total, jax.tree.map(lambda part, own: part[k].astype(own.dtype), pieces, value)
            )
            inside = jax.tree.map(lambda new, old: jnp.where(passed, new, old), total, inside)
        before = combine(inside, before)
    return before


def prefix_by_axis(value, axes, combine, identity):
    before = start = nothing_yet(value, identity)
    total = value
    for axis in reversed(axes):
        peers, mine = (lax.axis_size(axis), lax.axis_index(axis))
        pieces = lax.all_gather(total, axis)
        inside, total = (start, start)
        for k in reversed(range(peers)):
            passed = k > mine
            total = combine(total, pieces[k])
            inside = jnp.where(passed, total, inside)
        before = combine(inside, before)
    return before


def reduced_to_own(pieces, axes, order):
    inside = pieces.shape[1:]
    pieces = pieces.reshape(*(lax.axis_size(a) for a in axes), *inside)
    pieces = jnp.moveaxis(pieces, order, range(len(axes))).reshape(-1, *inside)
    for k in order:
        pieces = lax.psum_scatter(pieces, axes[k], scatter_dimension=0, tiled=True)
    return pieces[0]


def in_blocks(value, dim, peers):
    lengths = value.shape
    pieces = value.reshape(*lengths[:dim], peers, lengths[dim] // peers, *lengths[dim + 1 :])
    return jnp.moveaxis(pieces, dim, 0)


def summed_rows(value, axes, order, dim):
    peers = lax.axis_size(axes)
    return reduced_to_own(in_blocks(value, dim, peers), axes, order)


def layer_normed(tokens, norm_gain):
    values = tokens.astype(jnp.float32)
    center = values - jnp.mean(values, axis=-1, keepdims=True)
    spread = jnp.mean(center * center, axis=-1, keepdims=True)
    return (center * lax.rsqrt(spread + EPSILON) * norm_gain.astype(jnp.float32)).astype(
        jnp.bfloat16
    )


def gate_terms(query_sum, forget_sum, input_sum, floor_gap, extra_decay):
    query_raw = query_sum.astype(jnp.bfloat16)
    forget_raw = forget_sum.astype(jnp.bfloat16)
    input_raw = input_sum.astype(jnp.bfloat16)
    forget_pre = forget_raw.astype(jnp.float32)
    split_shape = forget_pre.shape[:-1] + (HEADS, HEAD)
    log_keep = jnp.logaddexp(
        jnp.log1p(-floor_gap), jnp.log(floor_gap) + jax.nn.log_sigmoid(forget_pre)
    )
    log_keep = log_keep.reshape(split_shape) + extra_decay[..., None]
    key_gate = (floor_gap * jax.nn.sigmoid(-forget_pre)).reshape(split_shape)
    query = jax.nn.silu(query_raw.astype(jnp.float32)).reshape(split_shape)
    values = input_raw.astype(jnp.float32).reshape(split_shape)
    return (query, key_gate, values, log_keep)


def block_pass(query, key_gate, values, log_keep):
    highest = lax.Precision.HIGHEST
    cumul = jnp.cumsum(log_keep, axis=2)
    q_decayed = query * jnp.exp(cumul)
    key_decayed = key_gate * jnp.exp(-cumul)
    causal = lax.broadcasted_iota(jnp.int32, (BLOCK, BLOCK), 0) >= lax.broadcasted_iota(
        jnp.int32, (BLOCK, BLOCK), 1
    )
    scores = jnp.einsum("snthd,snuhd->snhtu", q_decayed, key_decayed, precision=highest)
    scores = jnp.where(causal, scores, 0.0)
    within = jnp.einsum("snhtu,snuhe->snthe", scores, values, precision=highest)
    totals = cumul[:, :, -1]
    k_tail = key_gate * jnp.exp(totals[:, :, None] - cumul)
    block_state = jnp.einsum("snthd,snthe->snhde", k_tail, values, precision=highest)
    return (q_decayed, within, totals, block_state)


def linked_advance(earlier, later):
    return (earlier[0] + later[0], jnp.exp(later[0])[..., None] * earlier[1] + later[1])


def add_logs(earlier, later):
    return earlier + later


def read_out(q_global, leading_logarithm, prefix_state, init_part):
    carried = jnp.exp(leading_logarithm)[..., None] * init_part + prefix_state
    added = jnp.einsum("snthd,shde->snthe", q_global, carried, precision=lax.Precision.HIGHEST)
    return (carried, added)


def body(
    tokens,
    norm_gain,
    w_query,
    w_forget,
    w_input,
    floor_gap,
    extra_decay,
    init_state,
    head_norm_gain,
    w_output,
):
    normed = layer_normed(tokens, norm_gain)
    seqs, span = (tokens.shape[0], tokens.shape[1])

    def add_rows(piece):
        return jnp.dot(normed, piece, preferred_element_type=jnp.float32)

    query_sum = add_rows(lax.all_gather(w_query, "sp", axis=0, tiled=True))
    forget_sum = add_rows(lax.all_gather(w_forget, "sp", axis=0, tiled=True))
    input_sum = add_rows(lax.all_gather(w_input, "sp", axis=0, tiled=True))
    query, key_gate, values, log_keep = gate_terms(
        query_sum, forget_sum, input_sum, floor_gap, extra_decay
    )
    blocks = span // BLOCK
    blocked = (seqs, blocks, BLOCK, HEADS, HEAD)
    q_decayed, within, totals, block_state = block_pass(
        query.reshape(blocked),
        key_gate.reshape(blocked),
        values.reshape(blocked),
        log_keep.reshape(blocked),
    )
    running_state = jnp.zeros((seqs, HEADS, HEAD, HEAD), jnp.float32)
    running_log = jnp.zeros((seqs, HEADS, HEAD), jnp.float32)
    entering_list = []
    offset_list = []
    for number in range(blocks):
        entering_list.append(running_state)
        offset_list.append(running_log)
        running_state = (
            jnp.exp(totals[:, number])[..., None] * running_state + block_state[:, number]
        )
        running_log = running_log + totals[:, number]
    entering = jnp.stack(entering_list, axis=1)
    offsets = jnp.stack(offset_list, axis=1)
    local_out = within + jnp.einsum(
        "snthd,snhde->snthe", q_decayed, entering, precision=lax.Precision.HIGHEST
    )
    q_global = q_decayed * jnp.exp(offsets[:, :, None])
    leading_logarithm, prefix_state = entering_2(
        (running_log, running_state),
        SP_TP,
        linked_advance,
        (jnp.zeros_like(running_log), jnp.zeros_like(running_state)),
    )
    carried, added = read_out(q_global, leading_logarithm, prefix_state, init_state)
    flat_total = HEADS * HEAD * HEAD
    piece_count = flat_total // lax.axis_size(SP_TP)
    piece_start = lax.axis_index(SP_TP) * piece_count
    later_log = prefix_by_axis(running_log, SP_TP, add_logs, jnp.zeros_like(running_log))
    surviving = (jnp.exp(later_log)[..., None] * running_state).reshape(seqs, flat_total)
    summed = summed_rows(surviving.astype(jnp.bfloat16), SP_TP, (2, 0, 1), 1).astype(jnp.float32)
    initial_part = (
        jnp.exp(leading_logarithm + running_log + later_log)[..., None] * init_state
    ).reshape(seqs, flat_total)
    final_state = lax.dynamic_slice_in_dim(initial_part, piece_start, piece_count, 1) + summed
    recurrent = (local_out + added).reshape(seqs, span, HEADS, HEAD)
    average_power = jnp.mean(recurrent * recurrent, axis=-1, keepdims=True)
    scaled = (
        recurrent
        * lax.rsqrt(average_power + EPSILON)
        * head_norm_gain.astype(jnp.float32).reshape(HEADS, HEAD)
    )
    gated = scaled.reshape(seqs, span, HEADS * HEAD).astype(jnp.bfloat16)
    mixed = jnp.dot(
        gated,
        lax.all_gather(w_output, "sp", axis=1, tiled=True),
        preferred_element_type=jnp.float32,
    ).astype(jnp.bfloat16)
    return (mixed, final_state)


def solution(mesh):
    torus = Mesh(
        mesh.devices.reshape(mesh.shape["grp"], mesh.shape["sp"], 4, 2),
        ("grp", "sp", "tp_0", "tp_1"),
    )
    in_specs = (
        P("grp", SP_TP, None),
        P(),
        P("sp", None),
        P("sp", None),
        P("sp", None),
        P(),
        P("grp", SP_TP, None),
        P("grp", None, None, None),
        P(),
        P(None, "sp"),
    )
    out_specs = (P("grp", SP_TP, None), P("grp", SP_TP))
    return jax.shard_map(body, mesh=torus, in_specs=in_specs, out_specs=out_specs, check_vma=False)
```

profile of v0, /device:TPU:33, one launch (start us, length us, event | category | flops | bytes accessed | tf_op | source)
XLA Modules:
  0.0 580.1 jit_solution(18242492222280507001)
XLA Ops:
  7.2 0.7 all-gather.10.cloned.1.call-update
  8.0 0.7 all-gather.8.cloned.1.call-update
  8.8 0.7 all-gather.6.cloned.1.call-update
  9.7 0.7 convert_element_type.904
  10.4 0.8 copy.81
  11.2 1.2 convert_reduce_fusion
  12.4 1.3 fusion.7
  13.8 0.7 negate_log-plus-one_fusion
  14.5 77.2 %all-gather.10.cloned.1.call-done = bf16[2048,1024]{1,0:T(8,128)(2,1)} async-done(((bf16[128,1024]{1,0:T(8,128)(2,1)}), bf16[2048,1024]{1,0:T(8,128)(2,1)}) %all-gather.10.cloned.1.call-update) | async-done | bytes 4194320 | tf_op jit(solution)/shard_map/all_gather | solution.py:153
  91.7 3.8 add_select_fusion
  95.5 0.3 reshape.2012
  95.8 0.4 fusion.20
  96.3 11.2 %all_gather.51 = bf16[2,1,16,64]{3,2,1,0:T(8,128)(2,1)S(1)} all-gather(bf16[1,1,16,64]{3,2,1,0:T(8,128)(2,1)S(1)} %get-tuple-element.8), channel_id=1, replica_groups=mesh['grp'=2,'sp'=16,'tp_0'=4,'tp_1'=2] {'tp_1'}, dimensions={0}, use_global_device_ids=true | all-gather | bytes 6144 | tf_op jit(solution)/shard_map/all_gather | solution.py:28
  107.5 1.9 all_gather.58
  109.3 0.6 exponential_bitcast_fusion.1
  109.9 9.8 %all_gather.52 = bf16[4,1,16,64]{3,2,1,0:T(8,128)(2,1)S(1)} all-gather(bf16[1,1,16,64]{3,2,1,0:T(8,128)(2,1)S(1)} %get-tuple-element.47), channel_id=1, replica_groups=mesh['grp'=2,'sp'=16,'tp_0'=4,'tp_1'=2] {'tp_0'}, dimensions={0}, use_global_device_ids=true | all-gather | bytes 10240 | tf_op jit(solution)/shard_map/all_gather | solution.py:28
  119.7 9.6 %all_gather.59 = f32[4,1,16,64]{3,2,1,0:T(8,128)S(1)} all-gather(f32[1,1,16,64]{3,2,1,0:T(8,128)S(1)} %slice_add_fusion.18), channel_id=1, replica_groups=mesh['grp'=2,'sp'=16,'tp_0'=4,'tp_1'=2] {'tp_0'}, dimensions={0}, use_global_device_ids=true | all-gather | bytes 20480 | tf_op jit(solution)/shard_map/all_gather | solution.py:48
  129.4 25.1 %all_gather.53 = bf16[16,1,16,64]{3,2,1,0:T(8,128)(2,1)S(1)} all-gather(bf16[1,1,16,64]{3,2,1,0:T(8,128)(2,1)S(1)} %get-tuple-element.37), channel_id=1, replica_groups=mesh['grp'=2,'sp'=16,'tp_0'=4,'tp_1'=2] {'sp'}, dimensions={0}, use_global_device_ids=true | all-gather | bytes 34816 | tf_op jit(solution)/shard_map/all_gather | solution.py:28
  154.4 22.0 %all_gather.60 = f32[16,1,16,64]{3,2,1,0:T(8,128)S(1)} all-gather(f32[1,1,16,64]{3,2,1,0:T(8,128)S(1)} %slice_add_fusion.15), channel_id=1, replica_groups=mesh['grp'=2,'sp'=16,'tp_0'=4,'tp_1'=2] {'sp'}, dimensions={0}, use_global_device_ids=true | all-gather | bytes 69632 | tf_op jit(solution)/shard_map/all_gather | solution.py:48
  176.5 0.7 fusion.207
  177.1 0.2 mul.692
  177.3 0.2 mul.693
  177.6 1.3 reshape_reshape.8
  178.9 3.0 divide_multiply_fusion.1
  181.9 1.2 reshape_reshape.7
  183.2 58.4 %all-gather.6.cloned.1.call-done = bf16[2048,1024]{1,0:T(8,128)(2,1)} async-done(((bf16[128,1024]{1,0:T(8,128)(2,1)}), bf16[2048,1024]{1,0:T(8,128)(2,1)}) %all-gather.6.cloned.1.call-update) | async-done | bytes 4194320 | tf_op jit(solution)/shard_map/all_gather | solution.py:154
  241.6 3.0 convolution_convert_fusion.3
  244.5 0.3 reshape.2011
  244.9 3.3 fusion.16
  248.1 1.2 convolution_bitcast_fusion.1
  249.3 1.2 add_convert_fusion
  250.6 0.2 squeeze.40
  250.8 0.2 squeeze.41
  251.0 0.2 mul.694
  251.2 0.9 mul.695
  252.3 0.9 mul.697
  253.2 1.5 fusion.154
  254.8 0.7 reshape.2017
  255.7 11.9 %all_gather.54 = bf16[2,1,16,64,64]{4,3,2,1,0:T(8,128)(2,1)S(1)} all-gather(bf16[1,1,16,64,64]{4,3,2,1,0:T(8,128)(2,1)} %get-tuple-element.6), channel_id=1, replica_groups=mesh['grp'=2,'sp'=16,'tp_0'=4,'tp_1'=2] {'tp_1'}, dimensions={0}, use_global_device_ids=true | all-gather | bytes 393216 | tf_op jit(solution)/shard_map/all_gather | solution.py:28
  267.6 0.3 fusion.36
  267.9 13.5 %all_gather.55 = bf16[4,1,16,64,64]{4,3,2,1,0:T(8,128)(2,1)} all-gather(bf16[1,1,16,64,64]{4,3,2,1,0:T(8,128)(2,1)S(1)} %fusion.36), channel_id=1, replica_groups=mesh['grp'=2,'sp'=16,'tp_0'=4,'tp_1'=2] {'tp_0'}, dimensions={0}, use_global_device_ids=true | all-gather | bytes 655360 | tf_op jit(solution)/shard_map/all_gather | solution.py:28
  281.6 2.5 fusion.52
  284.2 0.7 all-gather.14.cloned.1.call-update
  284.9 1.3 dynamic-slice
  286.2 0.6 dynamic-slice.2
  286.8 0.6 convert_element_type.1001
  288.1 2.0 broadcast_multiply_fusion.1
  290.1 1.4 reshape.2016
  291.5 0.6 exp.348
  292.1 0.6 exp.349
  292.7 2.4 convolution_select_fusion
  295.1 1.0 fusion.96
  296.2 3.0 fusion.1
  299.3 103.4 %all-reduce.6.cloned.1.call-done = bf16[64,1,512]{2,0,1:T(8,128)(2,1)} async-done(((bf16[64,1,512]{2,0,1:T(8,128)(2,1)}), bf16[64,1,512]{2,0,1:T(8,128)(2,1)}) %all-reduce.6.cloned.1.call-update) | async-done | bytes 65552
  402.7 0.7 constant_dynamic-slice_fusion
  403.4 9.1 %all-reduce.3 = bf16[4,1,512]{2,0,1:T(4,128)(2,1)S(1)} all-reduce(bf16[4,1,512]{2,0,1:T(4,128)(2,1)S(1)} %constant_dynamic-slice_fusion), channel_id=4, replica_groups=mesh['grp'=2,'sp'=16,'tp_0'=4,'tp_1'=2] {'tp_0'}, use_global_device_ids=true, to_apply=%region_6.7.clone | all-reduce | flops 2048 | bytes 8192
  412.4 1.2 convert_add_fusion.55
  413.6 65.2 %all-gather.12.cloned.1.call-done = bf16[16,1,16,64,64]{4,3,2,1,0:T(8,128)(2,1)} async-done(((bf16[1,1,16,64,64]{4,3,2,1,0:T(8,128)(2,1)}), bf16[16,1,16,64,64]{4,3,2,1,0:T(8,128)(2,1)}) %all-gather.12.cloned.1.call-update) | async-done | bytes 2097168 | tf_op jit(solution)/shard_map/all_gather | solution.py:28
  478.9 10.3 %multiply_reduce_fusion = (f32[2,64,16]{1,2,0:T(8,128)S(1)}, f32[1,2,64,16,64]{2,4,3,1,0:T(8,128)}) fusion(f32[1,2,64,16,64]{2,4,3,1,0:T(8,128)} %fusion.1, f32[2,64,16,64]{3,2,1,0:T(8,128)S(1)} %copy-done.3, f32[1,16,64,64]{3,2,1,0:T(8,128)} %param.17, bf16[16,1,16,64,64]{4,3,2,1,0:T(8,128)(2,1)} %all-gather.12.cloned.1.call-done, ...), kind=kOutput, calls=%fused_computation.33 | convolution fusion | flops 107018240 | bytes 4829206 | tf_op jit(solution)/shard_map/snthd,shde->snthe/dot_general | solution.py:130
  489.2 1.7 copy.73
  490.9 0.3 reshape.2015
  491.4 0.2 copy.75
  491.6 77.9 %all-gather.14.cloned.1.call-done = bf16[1024,2048]{1,0:T(8,128)(2,1)} async-done(((bf16[1024,128]{1,0:T(8,128)(2,1)}), bf16[1024,2048]{1,0:T(8,128)(2,1)}) %all-gather.14.cloned.1.call-update) | async-done | bytes 4194320 | tf_op jit(solution)/shard_map/all_gather | solution.py:210
  569.5 3.7 fusion
  (64 shorter events, 1.2 us)
Async XLA Ops:
  7.2 84.5 %all-gather.10.cloned.1.call-start = ((), (), s32[]{:S(2)}) async-start(), calls=%async_computation.3 | async-start | bytes 4456448 | tf_op jit(solution)/shard_map/all_gather | solution.py:153
  8.0 170.9 %all-gather.8.cloned.1.call-start = ((), (), s32[]{:S(2)}) async-start(), calls=%async_computation.2 | async-start | bytes 4456448 | tf_op jit(solution)/shard_map/all_gather | solution.py:152
  8.8 232.8 %all-gather.6.cloned.1.call-start = ((), (), s32[]{:S(2)}) async-start(), calls=%async_computation.1 | async-start | bytes 4456448 | tf_op jit(solution)/shard_map/all_gather | solution.py:154
  9.6 271.9 %reduce-scatter.4.cloned.1.call-start = ((), (), s32[]{:S(2)}) async-start(), calls=%async_computation.6 | async-start | bytes 196608 | tf_op jit(solution)/shard_map/reduce_scatter | solution.py:63
  10.4 85.1 %copy-start.9 = (f32[2048]{0:T(1024)}, f32[2048]{0:T(1024)S(1)}, u32[]{:S(2)}) copy-start(f32[2048]{0:T(1024)S(1)} %convert_element_type.904) | copy-start | bytes 24580
  12.4 83.1 %copy-start.12 = (f32[128]{0:T(128)}, f32[128]{0:T(128)S(1)}, u32[]{:S(2)}) copy-start(f32[128]{0:T(128)S(1)} %broadcast_multiply_fusion.2) | copy-start | bytes 1540
  13.8 81.7 %copy-start.15 = (f32[128]{0:T(128)}, f32[128]{0:T(128)S(1)}, u32[]{:S(2)}) copy-start(f32[128]{0:T(128)S(1)} %add_rsqrt_fusion.1) | copy-start | bytes 1540
  95.5 83.3 %copy-start.1 = (bf16[1,128,2048]{2,1,0:T(8,128)(2,1)S(1)}, bf16[1,128,2048]{2,1,0:T(8,128)(2,1)}, u32[]{:S(2)}) copy-start(bf16[1,128,2048]{2,1,0:T(8,128)(2,1)} %param.10) | copy-start | bytes 1572868
  178.8 62.7 %copy-start.10 = (f32[2048]{0:T(1024)S(1)}, f32[2048]{0:T(1024)}, u32[]{:S(2)}) copy-start(f32[2048]{0:T(1024)} %copy-done.9) | copy-start | bytes 24580
  178.8 62.7 %copy-start.13 = (f32[128]{0:T(128)S(1)}, f32[128]{0:T(128)}, u32[]{:S(2)}) copy-start(f32[128]{0:T(128)} %copy-done.12) | copy-start | bytes 1540
  178.8 62.7 %copy-start.16 = (f32[128]{0:T(128)S(1)}, f32[128]{0:T(128)}, u32[]{:S(2)}) copy-start(f32[128]{0:T(128)} %copy-done.15) | copy-start | bytes 1540
  252.1 36.0 %copy-start.4 = (f32[16,64]{1,0:T(8,128)S(1)}, f32[16,64]{1,0:T(8,128)}, u32[]{:S(2)}) copy-start(f32[16,64]{1,0:T(8,128)} %get-tuple-element.2) | copy-start | bytes 12292
  252.3 33.9 %copy-start.14 = (u32[256]{0:T(256)S(1)}, u32[256]{0:T(256)}, u32[]{:S(2)}) copy-start(u32[256]{0:T(256)} %constant.88) | copy-start | bytes 3076
  252.3 34.5 %copy-start.11 = (bf16[1024]{0:T(1024)(128)(2,1)S(1)}, bf16[1024]{0:T(1024)(128)(2,1)}, u32[]{:S(2)}) copy-start(bf16[1024]{0:T(1024)(128)(2,1)} %param.18) | copy-start | bytes 6148
  253.2 38.3 %copy-start.6 = (f32[16,64]{1,0:T(8,128)S(1)}, f32[16,64]{1,0:T(8,128)}, u32[]{:S(2)}) copy-start(f32[16,64]{1,0:T(8,128)} %get-tuple-element.4) | copy-start | bytes 12292
  253.2 38.9 %copy-start.5 = (f32[16,64]{1,0:T(8,128)S(1)}, f32[16,64]{1,0:T(8,128)}, u32[]{:S(2)}) copy-start(f32[16,64]{1,0:T(8,128)} %get-tuple-element.5) | copy-start | bytes 12292
  253.2 39.5 %copy-start = (f32[2,64,16,64]{3,2,1,0:T(8,128)S(1)}, f32[2,64,16,64]{3,2,1,0:T(8,128)}, u32[]{:S(2)}) copy-start(f32[2,64,16,64]{3,2,1,0:T(8,128)} %get-tuple-element.13) | copy-start | bytes 1572868
  255.6 147.1 %all-reduce.6.cloned.1.call-start = ((), (), s32[]{:S(2)}) async-start(), calls=%async_computation.7 | async-start | bytes 131072
  281.5 197.3 %all-gather.12.cloned.1.call-start = ((), (), s32[]{:S(2)}) async-start(), calls=%async_computation.4 | async-start | bytes 4456448 | tf_op jit(solution)/shard_map/all_gather | solution.py:28
  284.1 285.4 %all-gather.14.cloned.1.call-start = ((), (), s32[]{:S(2)}) async-start(), calls=%async_computation.5 | async-start | bytes 4456448 | tf_op jit(solution)/shard_map/all_gather | solution.py:210
  291.5 4.7 copy-start.2
  292.7 186.1 %copy-start.8 = (f32[16,64]{1,0:T(8,128)S(1)}, f32[16,64]{1,0:T(8,128)}, u32[]{:S(2)}) copy-start(f32[16,64]{1,0:T(8,128)} %get-tuple-element.45) | copy-start | bytes 12292
  295.1 183.7 %copy-start.3 = (f32[2,64,16,64]{3,2,1,0:T(8,128)S(1)}, f32[2,64,16,64]{3,2,1,0:T(8,128)}, u32[]{:S(2)}) copy-start(f32[2,64,16,64]{3,2,1,0:T(8,128)} %get-tuple-element.16) | copy-start | bytes 1572868
  489.2 80.3 %copy-start.7 = (f32[1024]{0:T(1024)S(1)}, f32[1024]{0:T(1024)}, u32[]{:S(2)}) copy-start(f32[1024]{0:T(1024)} %convert_element_type.1001) | copy-start | bytes 12292
Sparse Core Ops, SparseCore 0:
  9.8 81.8 all-gather.9
  93.5 73.2 all-gather.7
  168.6 72.9 all-gather.5
  255.7 23.4 reduce-scatter.3
  281.6 120.9 all-reduce.5
  404.3 74.4 all-gather.11
  480.6 88.8 all-gather.13
where the time goes:
time: 589 us; the launch traced here: 580 us
  waiting for transfers between devices  385 us (65%)
  blocking collectives  114 us (19%)
  matrix products  31.4 us (5%)
  other arithmetic  18.4 us (3%)
  local copies, waits for them, and re-layouts  15.3 us (3%)
  between operations  15.3 us (3%)
    unnamed x8, waiting for transfers between devices  106 us
    all_gather x1, waiting for transfers between devices, body(): lax.all_gather(w_output, 'sp', axis=1, tiled=True)  77.9 us
    all_gather x1, waiting for transfers between devices, body(): forget_sum = add_rows(lax.all_gather(w_forget, 'sp', axis=0, tiled=True))  77.2 us
    all_gather x5, blocking collectives, entering_2(): lax.all_gather(part.astype(kind), axis)  71.5 us
    all_gather x1, waiting for transfers between devices, entering_2(): lax.all_gather(part.astype(kind), axis)  65.2 us
    all_gather x1, waiting for transfers between devices, body(): input_sum = add_rows(lax.all_gather(w_input, 'sp', axis=0, tiled=True))  58.4 us
    all_gather x3, blocking collectives, prefix_by_axis(): pieces = lax.all_gather(total, axis)  33.5 us
  transfers between devices with their start and end apart: 7, of which 5 were waited for; matrix products, arithmetic and copies ran while one was open for 8% of the time, Pallas kernels for 0%

commit v1 on v0

v1 whole, which is shorter than its diff:
```python
import jax
import jax.numpy as jnp
from jax import lax
from jax.experimental import pallas as pl
from jax.experimental.pallas import tpu as pltpu
from jax.sharding import PartitionSpec as P

HEADS = 16
HEAD = 64
BLOCK = 64
EPSILON = 1e-05
PIECES = 4
MESH = pl.DeviceIdType.MESH
BF = jnp.bfloat16
F32 = jnp.float32
NT = (((1,), (1,)), ((), ()))
TN = (((0,), (0,)), ((), ()))


def split3(value):
    high = value.astype(BF)
    rest = value - high.astype(F32)
    middle = rest.astype(BF)
    low = (rest - middle.astype(F32)).astype(BF)
    return high, middle, low


def mm(a, b, dims=None):
    if dims is None:
        return jnp.dot(a, b, preferred_element_type=F32)
    return lax.dot_general(a, b, dims, preferred_element_type=F32)


def make_kernel(n_sp, n_tp, span, width_own, d_model):
    half = n_sp // 2
    rows_all = n_tp * span
    n_blocks = rows_all // BLOCK
    piece_rows = span // PIECES
    piece_chunks = n_sp // PIECES
    k_rows = d_model // n_sp

    def kernel(
        tok_ref, gain_ref, wq_ref, wf_ref, wi_ref, gap_ref, ext_ref, init_ref, hgain_ref, wout_ref,
        mixed_ref, final_ref,
        tokens, weights, w_out, ext_all, pad, raw, keys, cums, entering, offsets, local_out, q_glob,
        own_state, states, gated, gated_in, final_buf, final_in, prefix,
        tok_send, tok_recv, wo_send, wo_recv, z_send, z_recv, ext_send, ext_recv,
        st_send, st_recv, g_send, g_recv, f_send, f_recv,
    ):
        s = lax.axis_index("sp")
        t = lax.axis_index("tp")
        chip, core = t // 2, t % 2
        n_chips = n_tp // 2
        right = ((chip + 1) % n_chips) * 2 + core
        left = ((chip + n_chips - 1) % n_chips) * 2 + core
        across = ((chip + 2) % n_chips) * 2 + core
        partner = chip * 2 + 1 - core
        up = (s + 1) % n_sp
        down = (s + n_sp - 1) % n_sp
        lanes = pl.ds(pl.multiple_of(t * width_own, width_own), width_own)

        def at_tp(index):
            return {"tp": index}

        def at_sp(index):
            return {"sp": index}

        sent = []

        def send(src, dst, send_sem, recv_sem, where):
            copy = pltpu.make_async_remote_copy(
                src_ref=src, dst_ref=dst, send_sem=send_sem, recv_sem=recv_sem,
                device_id=where, device_id_type=MESH,
            )
            copy.start()
            sent.append(copy)

        def arrived(dst, recv_sem):
            pltpu.make_async_remote_copy(
                src_ref=dst, dst_ref=dst, send_sem=tok_send.at[0], recv_sem=recv_sem,
                device_id=at_tp(partner), device_id_type=MESH,
            ).wait_recv()

        barrier = pltpu.get_barrier_semaphore()
        for i in range(1, n_tp):
            pl.semaphore_signal(
                barrier, inc=1, device_id=at_tp((t + i) % n_tp), device_id_type=MESH
            )
        for peer in (up, down):
            pl.semaphore_signal(barrier, inc=1, device_id=at_sp(peer), device_id_type=MESH)

        own_rows = pl.ds(pl.multiple_of(s * k_rows, k_rows), k_rows)
        for m, ref in enumerate((wq_ref, wf_ref, wi_ref)):
            weights[own_rows, m * width_own : (m + 1) * width_own] = ref[:, lanes]
        w_out[t, 0] = wout_ref[pl.ds(pl.multiple_of(t * width_own, width_own), width_own), :]
        pad[...] = jnp.zeros_like(pad)
        pad[:, :HEADS] = ext_ref[...]
        ext_all[t] = pad[...].T[:HEADS]

        pl.semaphore_wait(barrier, n_tp - 1 + 2)

        def z_piece(piece, source, slot):
            if piece < 3:
                rows = pl.ds(pl.multiple_of(source * k_rows, k_rows), k_rows)
                return weights.at[rows, pl.ds(piece * width_own, width_own)]
            return w_out.at[t, slot]

        def z_own(piece):
            if piece < 3:
                return (wq_ref, wf_ref, wi_ref)[piece].at[:, lanes]
            return wout_ref.at[pl.ds(pl.multiple_of(t * width_own, width_own), width_own), :]

        def z_pieces(direction, step):
            if step < half:
                return (1, 2, 0, 3)
            return (1, 0) if direction == 0 else (2, 3)

        def z_forward(step):
            for piece in (1, 2, 0, 3):
                for direction in (0, 1):
                    if piece not in z_pieces(direction, step):
                        continue
                    if direction == 0:
                        source = (s + n_sp - (step - 1)) % n_sp
                        slot_here, slot_there = max(2 * step - 3, 0), 2 * step - 1
                    else:
                        source = (s + (step - 1)) % n_sp
                        slot_here, slot_there = 2 * step - 2, min(2 * step, n_sp - 1)
                    src = z_own(piece) if step == 1 else z_piece(piece, source, slot_here)
                    send(
                        src, z_piece(piece, source, slot_there),
                        z_send.at[direction, step - 1, piece], z_recv.at[direction, step - 1, piece],
                        at_sp(up if direction == 0 else down),
                    )

        def z_arrived(step):
            for piece in (1, 2, 0, 3):
                for direction in (0, 1):
                    if piece not in z_pieces(direction, step):
                        continue
                    if direction == 0:
                        source, slot = (s + n_sp - step) % n_sp, 2 * step - 1
                    else:
                        source, slot = (s + step) % n_sp, min(2 * step, n_sp - 1)
                    arrived(z_piece(piece, source, slot), z_recv.at[direction, step - 1, piece])

        z_forward(1)

        for i in range(1, n_tp):
            send(
                ext_all.at[t], ext_all.at[t], ext_send.at[i], ext_recv.at[t],
                at_tp((t + i) % n_tp),
            )

        for p in range(PIECES):
            here = slice(p * piece_rows, (p + 1) * piece_rows)
            values = tok_ref[here, :].astype(F32)
            center = values - jnp.mean(values, axis=-1, keepdims=True)
            spread = jnp.mean(center * center, axis=-1, keepdims=True)
            normed = center * lax.rsqrt(spread + EPSILON) * gain_ref[...].astype(F32)
            tokens[pl.ds(pl.multiple_of(t * span + p * piece_rows, piece_rows), piece_rows), :] = (
                normed.astype(BF)
            )

        def tok_piece(block, p):
            return tokens.at[
                pl.ds(pl.multiple_of(block * span + p * piece_rows, piece_rows), piece_rows), :
            ]

        def wo_piece(block, p):
            return w_out.at[block, pl.ds(p * piece_chunks, piece_chunks)]

        class Ring:
            def __init__(self, piece, send_sem, recv_sem, left_first, onward):
                self.piece, self.send_sem, self.recv_sem = piece, send_sem, recv_sem
                self.count = 0
                onward_right, onward_left = onward
                self.onward_right, self.onward_left = onward_right, onward_left
                self.from_left = [(left, p) for p in range(PIECES)] + [
                    (across, p) for p in onward_right
                ]
                self.from_right = [(right, p) for p in left_first] + [
                    (across, p) for p in onward_left
                ]

            def push(self, block, p, where):
                send(
                    self.piece(block, p), self.piece(block, p),
                    self.send_sem.at[self.count], self.recv_sem.at[block, p], at_tp(where),
                )
                self.count += 1

            def take(self, j):
                for number, (block, p) in enumerate((self.from_left[j], self.from_right[j])):
                    arrived(self.piece(block, p), self.recv_sem.at[block, p])
                    if number == 0 and j < PIECES and p in self.onward_right:
                        self.push(block, p, right)
                    if number == 1 and j < PIECES and p in self.onward_left:
                        self.push(block, p, left)
                    self.push(block, p, partner)

            def partners(self):
                for where in (0, 1, n_chips - 1, 2):
                    block = ((chip + where) % n_chips) * 2 + 1 - core
                    for p in range(PIECES):
                        arrived(self.piece(block, p), self.recv_sem.at[block, p])

        tok_ring = Ring(tok_piece, tok_send, tok_recv, (2, 3, 0, 1), ((0, 1), (2, 3)))
        for p, q in zip((0, 1, 2, 3), (2, 3, 0, 1)):
            tok_ring.push(t, p, right)
            tok_ring.push(t, q, left)
        for p in range(PIECES):
            tok_ring.push(t, p, partner)
        wo_ring = Ring(wo_piece, wo_send, wo_recv, (0, 1, 2, 3), ((0, 1), (2, 3)))

        def wo_push(p):
            wo_ring.push(t, p, right)
            wo_ring.push(t, p, left)
            wo_ring.push(t, p, partner)

        ready = [((p + 1) * piece_chunks) // 2 for p in range(PIECES)]
        taken = 0
        for step in range(1, half + 1):
            z_arrived(step)
            if step < half:
                z_forward(step + 1)
            while taken < 6 and (taken < step or step == half):
                tok_ring.take(taken)
                taken += 1
            for p in range(PIECES):
                if ready[p] == step or (ready[p] == 0 and step == 1):
                    wo_push(p)
        tok_ring.partners()
        for i in range(1, n_tp):
            arrived(ext_all.at[(t + i) % n_tp], ext_recv.at[(t + i) % n_tp])

        rows_step = 256
        for r in range(0, rows_all, rows_step):
            raw[r : r + rows_step, :] = mm(tokens[r : r + rows_step, :], weights[...]).astype(BF)

        gap = gap_ref[:, lanes]
        row_i = lax.broadcasted_iota(jnp.int32, (2 * BLOCK, 2 * BLOCK), 0)
        col_i = lax.broadcasted_iota(jnp.int32, (2 * BLOCK, 2 * BLOCK), 1)
        causal = jnp.logical_and(row_i >= col_i, row_i // BLOCK == col_i // BLOCK)
        tri = jnp.where(causal, 1.0, 0.0).astype(BF)
        tri3 = jnp.concatenate([tri, tri, tri], axis=1)
        head_row = lax.broadcasted_iota(jnp.int32, (HEADS, width_own), 0)
        head_col = lax.broadcasted_iota(jnp.int32, (HEADS, width_own), 1)
        pick = jnp.where(
            head_row == t * (width_own // HEAD) + head_col // HEAD, 1.0, 0.0
        ).astype(BF)
        pick3 = jnp.concatenate([pick, pick, pick], axis=0)
        for i in range(n_tp):
            here = slice(i * span, (i + 1) * span)
            forget = raw[here, width_own : 2 * width_own].astype(F32)
            key = gap / (1.0 + jnp.exp(forget))
            extra = mm(jnp.concatenate(split3(ext_all[i]), axis=0), pick3, TN)
            log_keep = jnp.log1p(-key) + extra
            cums[here, :] = mm(tri3, jnp.concatenate(split3(log_keep), axis=0))
            keys[here, :] = key

        lane = lax.broadcasted_iota(jnp.int32, (HEAD, width_own), 1)
        first = lane < HEAD
        state = jnp.zeros((HEAD, width_own), F32)
        offset = jnp.zeros((1, width_own), F32)
        for b in range(n_blocks):
            here = slice(b * BLOCK, (b + 1) * BLOCK)
            total = cums[(b + 1) * BLOCK - 1 : (b + 1) * BLOCK, :]
            tail = (keys[here, :] * jnp.exp(total - cums[here, :])).astype(BF)
            added = mm(raw[here, 2 * width_own :], tail, TN)
            entering[b] = state.astype(BF)
            offsets[b] = offset
            state = state * jnp.exp(total) + jnp.where(first, added[:HEAD], added[HEAD:])
            offset = offset + total
        own_state[:HEAD] = state.astype(BF)
        o_high, o_middle, o_low = split3(offset)
        log_row = lax.broadcasted_iota(jnp.int32, (16, width_own), 0)
        own_state[HEAD:] = jnp.where(
            log_row == 0, o_high.astype(F32),
            jnp.where(log_row == 1, o_middle.astype(F32),
                      jnp.where(log_row == 2, o_low.astype(F32), 0.0)),
        ).astype(BF)
        states[s] = own_state[...]

        order = [half]
        for k in range(half - 1, 0, -1):
            order += [k, n_sp - k]
        for k in order:
            send(
                own_state, states.at[s], st_send.at[k], st_recv.at[s], at_sp((s + k) % n_sp),
            )

        for j in range(3):
            wo_ring.take(j)

        lane2 = lax.broadcasted_iota(jnp.int32, (span, width_own), 1)
        first2 = lane2 < HEAD

        def spread_heads(value, mask):
            zero = jnp.zeros_like(value)
            return jnp.concatenate(
                [jnp.where(mask, value, zero), jnp.where(mask, zero, value)], axis=0
            )

        for i in range(n_tp):
            here = slice(i * span, (i + 1) * span)
            query = raw[here, :width_own].astype(F32)
            query = query / (1.0 + jnp.exp(-query))
            cumul = cums[here, :]
            q_decayed = query * jnp.exp(cumul)
            k_decayed = (keys[here, :] * jnp.exp(-cumul)).astype(BF)
            scores = mm(spread_heads(q_decayed, first2).astype(BF), k_decayed, NT)
            scores = jnp.where(jnp.concatenate([causal, causal], axis=0), scores, 0.0)
            within = mm(scores.astype(BF), raw[here, 2 * width_own :])
            within = jnp.where(first2, within[:span], within[span:])
            for j in range(span // BLOCK):
                b = i * (span // BLOCK) + j
                part = slice(j * BLOCK, (j + 1) * BLOCK)
                q_part = q_decayed[part]
                seen = mm(
                    q_part.astype(BF), spread_heads(entering[b].astype(F32), first).astype(BF), NT
                )
                rows = slice(b * BLOCK, (b + 1) * BLOCK)
                local_out[rows, :] = within[part] + seen
                q_glob[rows, :] = (q_part * jnp.exp(offsets[b])).astype(BF)

        wo_ring.take(3)

        pad[...] = jnp.zeros_like(pad)
        pad[:, :HEAD] = init_ref[
            pl.ds(pl.multiple_of(t * width_own, width_own), width_own), :
        ]
        carried = pad[...].T[:HEAD]
        for k in range(1, n_sp):
            other = (s + k) % n_sp
            arrived(states.at[other], st_recv.at[other])

        def advance(j, value):
            logs = states[j, HEAD:].astype(F32)
            total = logs[0:1] + logs[1:2] + logs[2:3]
            return value * jnp.exp(total) + states[j, :HEAD].astype(F32)

        carried = lax.fori_loop(0, s, advance, carried)
        prefix[...] = spread_heads(carried, first).astype(BF)

        ones_row = lax.broadcasted_iota(jnp.int32, (width_own, width_own), 0)
        ones_col = lax.broadcasted_iota(jnp.int32, (width_own, width_own), 1)
        same = jnp.where(ones_row // HEAD == ones_col // HEAD, 1.0 / HEAD, 0.0).astype(BF)
        same2 = jnp.concatenate([same, same], axis=0)
        head_gain = hgain_ref[:, lanes].astype(F32)
        for i in range(1, n_tp + 1):
            block = (t + i) % n_tp
            rows = pl.ds(pl.multiple_of(block * span, span), span)
            recurrent = local_out[rows, :] + mm(q_glob[rows, :], prefix[...], NT)
            square = recurrent * recurrent
            high = square.astype(BF)
            low = (square - high.astype(F32)).astype(BF)
            power = mm(jnp.concatenate([high, low], axis=1), same2)
            done = (recurrent * lax.rsqrt(power + EPSILON) * head_gain).astype(BF)
            if i < n_tp:
                gated[rows, :] = done
                send(
                    gated.at[rows, :], gated_in.at[:, lanes], g_send.at[i], g_recv.at[t],
                    at_tp(block),
                )
            else:
                gated_in[:, lanes] = done

        if HEADS == n_sp:
            keeper = s // (HEADS // n_tp)
            sub = (s % (HEADS // n_tp)) * HEAD
            part_rows = HEAD // n_tp

            @pl.when(t == keeper)
            def _():
                last = lax.fori_loop(s, n_sp, advance, carried)
                turned = jnp.concatenate([last, last], axis=0).T
                final_buf[...] = turned
                final_in[...] = final_buf[
                    pl.ds(pl.multiple_of(sub + t * part_rows, part_rows), part_rows), :
                ]
                mine = []
                for i in range(1, n_tp):
                    other = (t + i) % n_tp
                    copy = pltpu.make_async_remote_copy(
                        src_ref=final_buf.at[
                            pl.ds(pl.multiple_of(sub + other * part_rows, part_rows), part_rows), :
                        ],
                        dst_ref=final_in, send_sem=f_send.at[i], recv_sem=f_recv,
                        device_id=at_tp(other), device_id_type=MESH,
                    )
                    copy.start()
                    mine.append(copy)
                for copy in mine:
                    copy.wait_send()

            @pl.when(t != keeper)
            def _():
                arrived(final_in, f_recv)

            for r in range(part_rows):
                final_ref[:, r * HEAD : (r + 1) * HEAD] = final_in[r : r + 1, :HEAD]

        wo_ring.take(4)
        wo_ring.take(5)
        wo_ring.partners()
        for i in range(1, n_tp):
            other = (t + i) % n_tp
            arrived(
                gated_in.at[:, pl.ds(pl.multiple_of(other * width_own, width_own), width_own)],
                g_recv.at[other],
            )

        def source_of(slot):
            step = (slot + 1) // 2
            return (s + n_sp - step) % n_sp if slot % 2 else (s + step) % n_sp

        for pair in range(n_sp // 2):
            right_side = jnp.concatenate(
                [w_out[:, slot].reshape(n_tp * width_own, -1) for slot in (2 * pair, 2 * pair + 1)],
                axis=1,
            )
            product = mm(gated_in[...], right_side).astype(BF)
            cols = product.shape[1] // 2
            for k in range(2):
                source = source_of(2 * pair + k)
                mixed_ref[:, pl.ds(pl.multiple_of(source * cols, cols), cols)] = (
                    product[:, k * cols : (k + 1) * cols]
                )
        for copy in sent:
            copy.wait_send()

    return kernel


def solution(mesh):
    n_sp, n_tp = mesh.shape["sp"], mesh.shape["tp"]

    def body(
        tokens, norm_gain, w_query, w_forget, w_input, floor_gap, extra_decay, init_state,
        head_norm_gain, w_output,
    ):
        span, d_model = tokens.shape[1], tokens.shape[2]
        width = w_query.shape[1]
        own = width // n_tp
        rows = n_tp * span
        blocks = rows // BLOCK
        flat = HEADS * HEAD * HEAD // (n_sp * n_tp)
        vmem = pl.BlockSpec(memory_space=pltpu.VMEM)
        dma = pltpu.SemaphoreType.DMA
        mixed, final_state = pl.pallas_call(
            make_kernel(n_sp, n_tp, span, own, d_model),
            out_shape=(
                jax.ShapeDtypeStruct((span, d_model), BF),
                jax.ShapeDtypeStruct((1, flat), F32),
            ),
            in_specs=[vmem] * 10,
            out_specs=(vmem, vmem),
            scratch_shapes=[
                pltpu.VMEM((rows, d_model), BF),
                pltpu.VMEM((d_model, 3 * own), BF),
                pltpu.VMEM((n_tp, n_sp, own, d_model // n_sp), BF),
                pltpu.VMEM((n_tp, HEADS, span), F32),
                pltpu.VMEM((span, own), F32),
                pltpu.VMEM((rows, 3 * own), BF),
                pltpu.VMEM((rows, own), F32),
                pltpu.VMEM((rows, own), F32),
                pltpu.VMEM((blocks, HEAD, own), BF),
                pltpu.VMEM((blocks, 1, own), F32),
                pltpu.VMEM((rows, own), F32),
                pltpu.VMEM((rows, own), BF),
                pltpu.VMEM((HEAD + 16, own), BF),
                pltpu.VMEM((n_sp, HEAD + 16, own), BF),
                pltpu.VMEM((rows, own), BF),
                pltpu.VMEM((span, width), BF),
                pltpu.VMEM((own, 2 * HEAD), F32),
                pltpu.VMEM((HEAD // n_tp, 2 * HEAD), F32),
                pltpu.VMEM((own, own), BF),
                dma((28,)), dma((n_tp, PIECES)), dma((28,)), dma((n_tp, PIECES)),
                dma((2, n_sp // 2, 4)), dma((2, n_sp // 2, 4)),
                dma((n_tp,)), dma((n_tp,)),
                dma((n_sp,)), dma((n_sp,)),
                dma((n_tp,)), dma((n_tp,)),
                dma((n_tp,)), dma,
            ],
            compiler_params=pltpu.CompilerParams(
                collective_id=0, has_side_effects=True, vmem_limit_bytes=56 * 1024 * 1024
            ),
            name="mixer",
        )(
            tokens.reshape(span, d_model),
            norm_gain.reshape(1, d_model),
            w_query, w_forget, w_input,
            floor_gap.reshape(1, width),
            extra_decay.reshape(span, HEADS),
            init_state.reshape(HEADS * HEAD, HEAD),
            head_norm_gain.reshape(1, width),
            w_output,
        )
        return mixed.reshape(1, span, d_model), final_state

    in_specs = (
        P("grp", ("sp", "tp"), None),
        P(),
        P("sp", None),
        P("sp", None),
        P("sp", None),
        P(),
        P("grp", ("sp", "tp"), None),
        P("grp", None, None, None),
        P(),
        P(None, "sp"),
    )
    out_specs = (P("grp", ("sp", "tp"), None), P("grp", ("sp", "tp")))
    return jax.shard_map(body, mesh=mesh, in_specs=in_specs, out_specs=out_specs, check_vma=False)
```

time: 589 us -> 99.1 us (0.17); the launches traced: 580 us -> 98.9 us
  waiting for transfers between devices: 385 us -> 0 us
  blocking collectives: 114 us -> 0 us
  Pallas kernels: 0 us -> 93.2 us
  matrix products: 31.4 us -> 0 us
  other arithmetic: 18.4 us -> 0 us
  between operations: 15.3 us -> 0.67 us
  local copies, waits for them, and re-layouts: 15.3 us -> 5.05 us
    all_gather x5 -> x0, waiting for transfers between devices: 279 us -> none  [the longest x1 77.9 us: body(): lax.all_gather(w_output, 'sp', axis=1, tiled=True)]
    unnamed x8 -> x0, waiting for transfers between devices: 106 us -> none
    all_gather x8 -> x0, blocking collectives: 105 us -> none  [the longest x5 71.5 us: entering_2(): lax.all_gather(part.astype(kind), axis)]
    pallas_call x0 -> x1, Pallas kernels: none -> 93.2 us  [body(): pl.pallas_call(make_kernel(n_sp, n_tp, span, own, d_model), out_shape=(ja...]
    dot_general x9 -> x0, matrix products: 31.4 us -> none  [the longest x1 10.3 us: read_out(): jnp.einsum('snthd,shde->snthe', q_global, carried, precision=lax.Precisio...]
    unnamed x1 -> x0, blocking collectives: 9.06 us -> none
  transfers between devices with their start and end apart: 7 -> 0, of which waited for: 5 -> 0; matrix products, arithmetic and copies ran while one was open for 8% -> 0% of each run, Pallas kernels for 0% -> 0%
where the time goes in v1:
time: 99.1 us; the launch traced here: 98.9 us
  Pallas kernels  93.2 us (94%)
  local copies, waits for them, and re-layouts  5.05 us (5%)
    pallas_call x1, Pallas kernels, body(): pl.pallas_call(make_kernel(n_sp, n_tp, span, own, d_model), out_shape=(ja...  93.2 us
    unnamed x11, local copies, waits for them, and re-layouts  3.87 us

profile of v1, /device:TPU:33, one launch (start us, length us, event | category | flops | bytes accessed | tf_op | source)
XLA Modules:
  0.0 98.9 jit_solution(13552487807927276870)
XLA Ops:
  0.6 0.0 copy-start.2
  0.6 0.0 copy-start.1
  0.7 0.7 copy-done.2
  1.3 0.0 copy-start
  1.3 0.6 reshape.30.hgain_ref
  1.9 0.0 copy-done.1
  1.9 0.6 reshape.26.gain_ref
  2.5 0.0 copy-done
  2.5 0.7 copy.12
  3.2 93.2 %mixer.1 = (bf16[128,2048]{1,0:T(8,128)(2,1)}, f32[1,512]{1,0:T(1,128)}) custom-call(bf16[128,2048]{1,0:T(8,128)(2,1)} %bitcast.6, bf16[1,2048]{1,0:T(2,128)(2,1)} %reshape.26.gain_ref, bf16[128,1024]{1,0:T(8,128)(2,1)} %wq_ref.1, bf16[128,1024]{1,0:T(8,128)(2,1)} %wf_ref.1, bf16[128,1024]{1,0:T(8,128)(2,1)} %wi_ref.1, f32[1,1024]{1,0:T(1,128)} %bitcast.9, ...), custom_call_target="tpu_custom_call" | custom-call | tf_op jit(solution)/shard_map/mixer/pallas_call | solution.py:451
  96.4 0.0 copy-start.3
  96.4 1.9 %copy.15 = bf16[1,128,2048]{2,1,0:T(8,128)(2,1)} copy(bf16[1,128,2048]{2,1,0:T(8,128)(2,1)} %bitcast.5) | data formatting | bytes 1048576
  98.3 0.0 copy-done.3
  98.3 0.6 copy.16
Async XLA Ops:
  0.6 0.7 copy-start.2
  0.6 1.3 %copy-start.1 = (bf16[2048]{0:T(1024)(128)(2,1)S(1)}, bf16[2048]{0:T(1024)(128)(2,1)}, u32[]{:S(2)}) copy-start(bf16[2048]{0:T(1024)(128)(2,1)} %param.11) | copy-start | bytes 12292
  1.3 1.2 %copy-start = (f32[1,128,16]{1,2,0:T(8,128)S(1)}, f32[1,128,16]{1,2,0:T(8,128)}, u32[]{:S(2)}) copy-start(f32[1,128,16]{1,2,0:T(8,128)} %param.16) | copy-start | bytes 24580
  96.4 1.9 %copy-start.3 = (f32[1,512]{1,0:T(1,128)S(1)}, f32[1,512]{1,0:T(1,128)}, u32[]{:S(2)}) copy-start(f32[1,512]{1,0:T(1,128)} %get-tuple-element.9) | copy-start | bytes 6148

commit v2 on v1

--- a/solution.py
+++ b/solution.py
@@ -10,6 +10,8 @@
 BLOCK = 64
 EPSILON = 1e-05
 PIECES = 4
+LAG = 2
+LOG_ROWS = 8
 MESH = pl.DeviceIdType.MESH
 BF = jnp.bfloat16
 F32 = jnp.float32
@@ -42,9 +44,10 @@
     def kernel(
         tok_ref, gain_ref, wq_ref, wf_ref, wi_ref, gap_ref, ext_ref, init_ref, hgain_ref, wout_ref,
         mixed_ref, final_ref,
-        tokens, weights, w_out, ext_all, pad, raw, keys, cums, entering, offsets, local_out, q_glob,
-        own_state, states, gated, gated_in, final_buf, final_in, prefix,
-        tok_send, tok_recv, wo_send, wo_recv, z_send, z_recv, ext_send, ext_recv,
+        tok_in, init_in, tokens, weights, others, w_out, ext_all, pad, raw, keys, cums, entering,
+        offsets, local_out, q_glob, own_state, states, gated, gated_in, final_buf, final_in, prefix,
+        load_sem, tok_send, tok_recv, wo_send, wo_recv, z_send, z_recv, zo_send, zo_recv,
+        d_send, d_recv, do_send, do_recv, ext_send, ext_recv,
         st_send, st_recv, g_send, g_recv, f_send, f_recv,
     ):
         s = lax.axis_index("sp")
@@ -55,9 +58,10 @@
         left = ((chip + n_chips - 1) % n_chips) * 2 + core
         across = ((chip + 2) % n_chips) * 2 + core
         partner = chip * 2 + 1 - core
-        up = (s + 1) % n_sp
-        down = (s + n_sp - 1) % n_sp
+        onto = (s + n_sp + 1 - 2 * core) % n_sp
+        behind = (s + n_sp - 1 + 2 * core) % n_sp
         lanes = pl.ds(pl.multiple_of(t * width_own, width_own), width_own)
+        lanes_partner = pl.ds(pl.multiple_of(partner * width_own, width_own), width_own)
 
         def at_tp(index):
             return {"tp": index}
@@ -86,81 +90,112 @@
             pl.semaphore_signal(
                 barrier, inc=1, device_id=at_tp((t + i) % n_tp), device_id_type=MESH
             )
-        for peer in (up, down):
-            pl.semaphore_signal(barrier, inc=1, device_id=at_sp(peer), device_id_type=MESH)
-
-        own_rows = pl.ds(pl.multiple_of(s * k_rows, k_rows), k_rows)
+        pl.semaphore_signal(barrier, inc=1, device_id=at_sp(behind), device_id_type=MESH)
+
+        def source_at(step):
+            return (s + n_sp - step + 2 * core * step) % n_sp
+
+        def source_beside(step):
+            return (s + n_sp + step - 2 * core * step) % n_sp
+
+        def slot_at(step):
+            if step == 0:
+                return 0
+            return n_sp - 1 if step == half else 2 * step - 1 + core
+
+        def w_piece(ref, source, m):
+            rows = pl.ds(pl.multiple_of(source * k_rows, k_rows), k_rows)
+            return ref.at[rows, pl.ds(m * width_own, width_own)]
+
+        def own_channels(index):
+            return pl.ds(pl.multiple_of(index * width_own, width_own), width_own)
+
+        loads = []
+
+        def load(src, dst):
+            copy = pltpu.make_async_copy(src, dst, load_sem.at[len(loads)])
+            copy.start()
+            loads.append(copy)
+
+        load(tok_ref, tok_in)
         for m, ref in enumerate((wq_ref, wf_ref, wi_ref)):
-            weights[own_rows, m * width_own : (m + 1) * width_own] = ref[:, lanes]
-        w_out[t, 0] = wout_ref[pl.ds(pl.multiple_of(t * width_own, width_own), width_own), :]
-        pad[...] = jnp.zeros_like(pad)
-        pad[:, :HEADS] = ext_ref[...]
-        ext_all[t] = pad[...].T[:HEADS]
-
-        pl.semaphore_wait(barrier, n_tp - 1 + 2)
-
-        def z_piece(piece, source, slot):
-            if piece < 3:
-                rows = pl.ds(pl.multiple_of(source * k_rows, k_rows), k_rows)
-                return weights.at[rows, pl.ds(piece * width_own, width_own)]
-            return w_out.at[t, slot]
-
-        def z_own(piece):
-            if piece < 3:
-                return (wq_ref, wf_ref, wi_ref)[piece].at[:, lanes]
-            return wout_ref.at[pl.ds(pl.multiple_of(t * width_own, width_own), width_own), :]
-
-        def z_pieces(direction, step):
-            if step < half:
-                return (1, 2, 0, 3)
-            return (1, 0) if direction == 0 else (2, 3)
-
-        def z_forward(step):
-            for piece in (1, 2, 0, 3):
-                for direction in (0, 1):
-                    if piece not in z_pieces(direction, step):
-                        continue
-                    if direction == 0:
-                        source = (s + n_sp - (step - 1)) % n_sp
-                        slot_here, slot_there = max(2 * step - 3, 0), 2 * step - 1
-                    else:
-                        source = (s + (step - 1)) % n_sp
-                        slot_here, slot_there = 2 * step - 2, min(2 * step, n_sp - 1)
-                    src = z_own(piece) if step == 1 else z_piece(piece, source, slot_here)
-                    send(
-                        src, z_piece(piece, source, slot_there),
-                        z_send.at[direction, step - 1, piece], z_recv.at[direction, step - 1, piece],
-                        at_sp(up if direction == 0 else down),
-                    )
-
-        def z_arrived(step):
-            for piece in (1, 2, 0, 3):
-                for direction in (0, 1):
-                    if piece not in z_pieces(direction, step):
-                        continue
-                    if direction == 0:
-                        source, slot = (s + n_sp - step) % n_sp, 2 * step - 1
-                    else:
-                        source, slot = (s + step) % n_sp, min(2 * step, n_sp - 1)
-                    arrived(z_piece(piece, source, slot), z_recv.at[direction, step - 1, piece])
-
-        z_forward(1)
-
-        for i in range(1, n_tp):
-            send(
-                ext_all.at[t], ext_all.at[t], ext_send.at[i], ext_recv.at[t],
-                at_tp((t + i) % n_tp),
-            )
-
+            load(ref.at[:, lanes_partner], w_piece(others, s, m))
+            load(ref.at[:, lanes], w_piece(weights, s, m))
+        load(ext_ref, ext_all.at[t])
+        load(wout_ref.at[own_channels(t), :], w_out.at[t, 0])
+        load(wout_ref.at[own_channels(partner), :], w_out.at[partner, 0])
+        load(init_ref.at[own_channels(t), :], init_in)
+
+        loads[0].wait()
+        gain = gain_ref[...].astype(F32).reshape(1, d_model)
         for p in range(PIECES):
             here = slice(p * piece_rows, (p + 1) * piece_rows)
-            values = tok_ref[here, :].astype(F32)
+            values = tok_in[here, :].astype(F32)
             center = values - jnp.mean(values, axis=-1, keepdims=True)
             spread = jnp.mean(center * center, axis=-1, keepdims=True)
-            normed = center * lax.rsqrt(spread + EPSILON) * gain_ref[...].astype(F32)
+            normed = center * lax.rsqrt(spread + EPSILON) * gain
             tokens[pl.ds(pl.multiple_of(t * span + p * piece_rows, piece_rows), piece_rows), :] = (
                 normed.astype(BF)
             )
+        for copy in loads[1:]:
+            copy.wait()
+
+        pl.semaphore_wait(barrier, n_tp - 1 + 1)
+
+        def z_items(step):
+            return [(m, part) for m in (1, 2, 0) for part in ((1, 0) if step < half else (0,))]
+
+        def z_push(step, m, part):
+            ref = others if part else weights
+            piece = w_piece(ref, source_at(step - 1), m)
+            send(
+                piece, piece, z_send.at[step - 1, m, part], z_recv.at[step - 1, m, part],
+                at_sp(onto),
+            )
+
+        def z_step(step):
+            for m, part in z_items(step):
+                piece = w_piece(others if part else weights, source_at(step), m)
+                arrived(piece, z_recv.at[step - 1, m, part])
+                if step < half and (m, part) in z_items(step + 1):
+                    z_push(step + 1, m, part)
+                if part:
+                    send(
+                        piece, w_piece(weights, source_at(step), m), d_send.at[step - 1, m],
+                        d_recv.at[step - 1, m], at_tp(partner),
+                    )
+
+        def zo_parts(step):
+            return (1, 0) if step < half else (0,)
+
+        def zo_push(step, part):
+            block = partner if part else t
+            send(
+                w_out.at[block, slot_at(step - 1)], w_out.at[block, slot_at(step)],
+                zo_send.at[step - 1, part], zo_recv.at[step - 1, part], at_sp(onto),
+            )
+
+        def zo_step(step):
+            if step == 0:
+                for part in (1, 0):
+                    zo_push(1, part)
+                return
+            for part in zo_parts(step):
+                piece = w_out.at[partner if part else t, slot_at(step)]
+                arrived(piece, zo_recv.at[step - 1, part])
+                if step < half and part in zo_parts(step + 1):
+                    zo_push(step + 1, part)
+                send(
+                    piece, piece, do_send.at[step - 1, part], do_recv.at[step - 1, part],
+                    at_tp(partner),
+                )
+
+        def zo_beside(step, part):
+            slot = n_sp - 1 if step == half else 2 * step - core
+            arrived(w_out.at[t if part else partner, slot], do_recv.at[step - 1, part])
+
+        for m, part in z_items(1):
+            z_push(1, m, part)
 
         def tok_piece(block, p):
             return tokens.at[
@@ -199,12 +234,17 @@
                         self.push(block, p, left)
                     self.push(block, p, partner)
 
-            def partners(self):
-                for where in (0, 1, n_chips - 1, 2):
+            def partners(self, chips):
+                for where in chips:
                     block = ((chip + where) % n_chips) * 2 + 1 - core
                     for p in range(PIECES):
                         arrived(self.piece(block, p), self.recv_sem.at[block, p])
 
+        for i in range(1, n_tp):
+            send(
+                ext_all.at[t], ext_all.at[t], ext_send.at[i], ext_recv.at[t],
+                at_tp((t + i) % n_tp),
+            )
         tok_ring = Ring(tok_piece, tok_send, tok_recv, (2, 3, 0, 1), ((0, 1), (2, 3)))
         for p, q in zip((0, 1, 2, 3), (2, 3, 0, 1)):
             tok_ring.push(t, p, right)
@@ -213,24 +253,33 @@
             tok_ring.push(t, p, partner)
         wo_ring = Ring(wo_piece, wo_send, wo_recv, (0, 1, 2, 3), ((0, 1), (2, 3)))
 
-        def wo_push(p):
-            wo_ring.push(t, p, right)
-            wo_ring.push(t, p, left)
-            wo_ring.push(t, p, partner)
-
         ready = [((p + 1) * piece_chunks) // 2 for p in range(PIECES)]
+        pushed = [0, 0]
+
+        def wo_advance(step):
+            while pushed[0] < PIECES and ready[pushed[0]] < step:
+                while pushed[1] < ready[pushed[0]]:
+                    pushed[1] += 1
+                    for part in reversed(zo_parts(pushed[1])):
+                        zo_beside(pushed[1], part)
+                wo_ring.push(t, pushed[0], right)
+                wo_ring.push(t, pushed[0], left)
+                pushed[0] += 1
+            if step <= half:
+                zo_step(step)
+
         taken = 0
         for step in range(1, half + 1):
-            z_arrived(step)
-            if step < half:
-                z_forward(step + 1)
+            z_step(step)
             while taken < 6 and (taken < step or step == half):
                 tok_ring.take(taken)
                 taken += 1
-            for p in range(PIECES):
-                if ready[p] == step or (ready[p] == 0 and step == 1):
-                    wo_push(p)
-        tok_ring.partners()
+            if step >= LAG:
+                wo_advance(step - LAG)
+        for step in range(1, half):
+            for m in range(3):
+                arrived(w_piece(weights, source_beside(step), m), d_recv.at[step - 1, m])
+        tok_ring.partners((0, 1, n_chips - 1, 2))
         for i in range(1, n_tp):
             arrived(ext_all.at[(t + i) % n_tp], ext_recv.at[(t + i) % n_tp])
 
@@ -238,6 +287,7 @@
         for r in range(0, rows_all, rows_step):
             raw[r : r + rows_step, :] = mm(tokens[r : r + rows_step, :], weights[...]).astype(BF)
 
+        wo_advance(half - LAG + 1)
         gap = gap_ref[:, lanes]
         row_i = lax.broadcasted_iota(jnp.int32, (2 * BLOCK, 2 * BLOCK), 0)
         col_i = lax.broadcasted_iota(jnp.int32, (2 * BLOCK, 2 * BLOCK), 1)
@@ -274,25 +324,28 @@
             offset = offset + total
         own_state[:HEAD] = state.astype(BF)
         o_high, o_middle, o_low = split3(offset)
-        log_row = lax.broadcasted_iota(jnp.int32, (16, width_own), 0)
+        log_row = lax.broadcasted_iota(jnp.int32, (LOG_ROWS, width_own), 0)
         own_state[HEAD:] = jnp.where(
             log_row == 0, o_high.astype(F32),
             jnp.where(log_row == 1, o_middle.astype(F32),
                       jnp.where(log_row == 2, o_low.astype(F32), 0.0)),
         ).astype(BF)
-        states[s] = own_state[...]
-
-        order = [half]
-        for k in range(half - 1, 0, -1):
-            order += [k, n_sp - k]
-        for k in order:
-            send(
-                own_state, states.at[s], st_send.at[k], st_recv.at[s], at_sp((s + k) % n_sp),
-            )
-
-        for j in range(3):
+
+        def state_copy(j):
+            return pltpu.make_async_remote_copy(
+                src_ref=own_state, dst_ref=states.at[s], send_sem=st_send.at[j],
+                recv_sem=st_recv.at[s], device_id=at_sp(j), device_id_type=MESH,
+            )
+
+        def state_push(k, carry):
+            state_copy(n_sp - 1 - k).start()
+            return carry
+
+        lax.fori_loop(0, n_sp - 1 - s, state_push, 0)
+        for step in range(half - LAG + 2, half + 2):
+            wo_advance(step)
+        for j in range(2):
             wo_ring.take(j)
-
         lane2 = lax.broadcasted_iota(jnp.int32, (span, width_own), 1)
         first2 = lane2 < HEAD
 
@@ -324,18 +377,15 @@
                 local_out[rows, :] = within[part] + seen
                 q_glob[rows, :] = (q_part * jnp.exp(offsets[b])).astype(BF)
 
+        wo_ring.take(2)
         wo_ring.take(3)
 
         pad[...] = jnp.zeros_like(pad)
-        pad[:, :HEAD] = init_ref[
-            pl.ds(pl.multiple_of(t * width_own, width_own), width_own), :
-        ]
+        pad[:, :HEAD] = init_in[...]
         carried = pad[...].T[:HEAD]
-        for k in range(1, n_sp):
-            other = (s + k) % n_sp
-            arrived(states.at[other], st_recv.at[other])
 
         def advance(j, value):
+            arrived(states.at[j], st_recv.at[j])
             logs = states[j, HEAD:].astype(F32)
             total = logs[0:1] + logs[1:2] + logs[2:3]
             return value * jnp.exp(total) + states[j, :HEAD].astype(F32)
@@ -347,7 +397,10 @@
         ones_col = lax.broadcasted_iota(jnp.int32, (width_own, width_own), 1)
         same = jnp.where(ones_row // HEAD == ones_col // HEAD, 1.0 / HEAD, 0.0).astype(BF)
         same2 = jnp.concatenate([same, same], axis=0)
-        head_gain = hgain_ref[:, lanes].astype(F32)
+        gains = hgain_ref[...].astype(F32).reshape(1, n_tp * width_own)
+        head_gain = gains[:, :width_own]
+        for i in range(1, n_tp):
+            head_gain = jnp.where(t == i, gains[:, i * width_own : (i + 1) * width_own], head_gain)
         for i in range(1, n_tp + 1):
             block = (t + i) % n_tp
             rows = pl.ds(pl.multiple_of(block * span, span), span)
@@ -366,44 +419,44 @@
             else:
                 gated_in[:, lanes] = done
 
+        part_rows = HEAD // n_tp
+
+        def final_copies(act):
+            for h in range(HEADS // n_tp):
+                head = t * (HEADS // n_tp) + h
+                for i in range(n_tp):
+                    copy = pltpu.make_async_remote_copy(
+                        src_ref=final_buf.at[pl.ds(h * HEAD + i * part_rows, part_rows), :],
+                        dst_ref=final_in, send_sem=f_send.at[h, i], recv_sem=f_recv,
+                        device_id={"sp": head, "tp": i}, device_id_type=MESH,
+                    )
+                    keeps = jnp.logical_and(head == s, t == i)
+                    if act == "start":
+                        pl.when(jnp.logical_not(keeps))(copy.start)
+
+                        @pl.when(keeps)
+                        def _():
+                            final_in[...] = final_buf[
+                                h * HEAD + i * part_rows : h * HEAD + (i + 1) * part_rows, :
+                            ]
+                    else:
+                        pl.when(jnp.logical_not(keeps))(copy.wait_send)
+
         if HEADS == n_sp:
-            keeper = s // (HEADS // n_tp)
-            sub = (s % (HEADS // n_tp)) * HEAD
-            part_rows = HEAD // n_tp
-
-            @pl.when(t == keeper)
+
+            @pl.when(s == n_sp - 1)
             def _():
-                last = lax.fori_loop(s, n_sp, advance, carried)
-                turned = jnp.concatenate([last, last], axis=0).T
-                final_buf[...] = turned
-                final_in[...] = final_buf[
-                    pl.ds(pl.multiple_of(sub + t * part_rows, part_rows), part_rows), :
-                ]
-                mine = []
-                for i in range(1, n_tp):
-                    other = (t + i) % n_tp
-                    copy = pltpu.make_async_remote_copy(
-                        src_ref=final_buf.at[
-                            pl.ds(pl.multiple_of(sub + other * part_rows, part_rows), part_rows), :
-                        ],
-                        dst_ref=final_in, send_sem=f_send.at[i], recv_sem=f_recv,
-                        device_id=at_tp(other), device_id_type=MESH,
-                    )
-                    copy.start()
-                    mine.append(copy)
-                for copy in mine:
-                    copy.wait_send()
-
-            @pl.when(t != keeper)
-            def _():
-                arrived(final_in, f_recv)
-
-            for r in range(part_rows):
-                final_ref[:, r * HEAD : (r + 1) * HEAD] = final_in[r : r + 1, :HEAD]
+                last = carried * jnp.exp(offset) + state
+                final_buf[...] = jnp.concatenate([last, last], axis=0).T
+                final_copies("start")
 
         wo_ring.take(4)
         wo_ring.take(5)
-        wo_ring.partners()
+        wo_ring.partners((1, n_chips - 1, 2))
+        for step in range(1, half + 1):
+            for part in zo_parts(step):
+                if step > pushed[1]:
+                    zo_beside(step, part)
         for i in range(1, n_tp):
             other = (t + i) % n_tp
             arrived(
@@ -427,6 +480,26 @@
                 mixed_ref[:, pl.ds(pl.multiple_of(source * cols, cols), cols)] = (
                     product[:, k * cols : (k + 1) * cols]
                 )
+        if HEADS == n_sp:
+
+            @pl.when(s == n_sp - 1)
+            def _():
+                final_copies("end")
+
+            keeper = jnp.logical_and(s == n_sp - 1, t == s // (HEADS // n_tp))
+
+            @pl.when(jnp.logical_not(keeper))
+            def _():
+                arrived(final_in, f_recv)
+
+            for r in range(part_rows):
+                final_ref[:, r * HEAD : (r + 1) * HEAD] = final_in[r : r + 1, :HEAD]
+
+        def state_end(k, carry):
+            state_copy(n_sp - 1 - k).wait_send()
+            return carry
+
+        lax.fori_loop(0, n_sp - 1 - s, state_end, 0)
         for copy in sent:
             copy.wait_send()
 
@@ -447,6 +520,8 @@
         blocks = rows // BLOCK
         flat = HEADS * HEAD * HEAD // (n_sp * n_tp)
         vmem = pl.BlockSpec(memory_space=pltpu.VMEM)
+        hbm = pl.BlockSpec(memory_space=pl.ANY)
+        half = n_sp // 2
         dma = pltpu.SemaphoreType.DMA
         mixed, final_state = pl.pallas_call(
             make_kernel(n_sp, n_tp, span, own, d_model),
@@ -454,10 +529,13 @@
                 jax.ShapeDtypeStruct((span, d_model), BF),
                 jax.ShapeDtypeStruct((1, flat), F32),
             ),
-            in_specs=[vmem] * 10,
+            in_specs=[hbm, vmem, hbm, hbm, hbm, vmem, hbm, hbm, vmem, hbm],
             out_specs=(vmem, vmem),
             scratch_shapes=[
+                pltpu.VMEM((span, d_model), BF),
+                pltpu.VMEM((own, HEAD), F32),
                 pltpu.VMEM((rows, d_model), BF),
+                pltpu.VMEM((d_model, 3 * own), BF),
                 pltpu.VMEM((d_model, 3 * own), BF),
                 pltpu.VMEM((n_tp, n_sp, own, d_model // n_sp), BF),
                 pltpu.VMEM((n_tp, HEADS, span), F32),
@@ -469,19 +547,21 @@
                 pltpu.VMEM((blocks, 1, own), F32),
                 pltpu.VMEM((rows, own), F32),
                 pltpu.VMEM((rows, own), BF),
-                pltpu.VMEM((HEAD + 16, own), BF),
-                pltpu.VMEM((n_sp, HEAD + 16, own), BF),
+                pltpu.VMEM((HEAD + LOG_ROWS, own), BF),
+                pltpu.VMEM((n_sp, HEAD + LOG_ROWS, own), BF),
                 pltpu.VMEM((rows, own), BF),
                 pltpu.VMEM((span, width), BF),
                 pltpu.VMEM((own, 2 * HEAD), F32),
                 pltpu.VMEM((HEAD // n_tp, 2 * HEAD), F32),
                 pltpu.VMEM((own, own), BF),
+                dma((11,)),
                 dma((28,)), dma((n_tp, PIECES)), dma((28,)), dma((n_tp, PIECES)),
-                dma((2, n_sp // 2, 4)), dma((2, n_sp // 2, 4)),
+                dma((half, 3, 2)), dma((half, 3, 2)), dma((half, 2)), dma((half, 2)),
+                dma((half, 3)), dma((half, 3)), dma((half, 2)), dma((half, 2)),
                 dma((n_tp,)), dma((n_tp,)),
                 dma((n_sp,)), dma((n_sp,)),
                 dma((n_tp,)), dma((n_tp,)),
-                dma((n_tp,)), dma,
+                dma((HEADS // n_tp, n_tp)), dma,
             ],
             compiler_params=pltpu.CompilerParams(
                 collective_id=0, has_side_effects=True, vmem_limit_bytes=56 * 1024 * 1024
@@ -489,12 +569,12 @@
             name="mixer",
         )(
             tokens.reshape(span, d_model),
-            norm_gain.reshape(1, d_model),
+            norm_gain,
             w_query, w_forget, w_input,
             floor_gap.reshape(1, width),
-            extra_decay.reshape(span, HEADS),
+            jnp.swapaxes(extra_decay, 1, 2).reshape(HEADS, span),
             init_state.reshape(HEADS * HEAD, HEAD),
-            head_norm_gain.reshape(1, width),
+            head_norm_gain,
             w_output,
         )
         return mixed.reshape(1, span, d_model), final_state

time: 99.1 us -> 83.7 us (0.84)
  Pallas kernels: 93.2 us -> 80.4 us
  local copies, waits for them, and re-layouts: 5.05 us -> 2.46 us
    pallas_call x1, Pallas kernels: 93.2 us -> 80.4 us  [body(): pl.pallas_call(make_kernel(n_sp, n_tp, span, own, d_model), out_shape=(ja...]
    unnamed x11 -> x4, local copies, waits for them, and re-layouts: 3.87 us -> 2.46 us
    reshape x2 -> x0, local copies, waits for them, and re-layouts: 1.18 us -> none  [the longest x1 0.6 us: body(): norm_gain.reshape(1, d_model)]
where the time goes in v2:
time: 83.7 us; the launch traced here: 83.5 us
  Pallas kernels  80.4 us (96%)
  local copies, waits for them, and re-layouts  2.46 us (3%)
    pallas_call x1, Pallas kernels, body(): pl.pallas_call(make_kernel(n_sp, n_tp, span, own, d_model), out_shape=(ja...  80.4 us
    unnamed x4, local copies, waits for them, and re-layouts  2.46 us

profile of v2, /device:TPU:33, one launch (start us, length us, event | category | flops | bytes accessed | tf_op | source)
XLA Modules:
  0.0 83.5 jit_solution(1905148618598271811)
XLA Ops:
  0.6 80.4 %mixer.1 = (bf16[128,2048]{1,0:T(8,128)(2,1)}, f32[1,512]{1,0:T(1,128)}) custom-call(bf16[128,2048]{1,0:T(8,128)(2,1)} %bitcast.7, bf16[2048]{0:T(1024)(128)(2,1)} %gain_ref.1, bf16[128,1024]{1,0:T(8,128)(2,1)} %wq_ref.1, bf16[128,1024]{1,0:T(8,128)(2,1)} %wf_ref.1, bf16[128,1024]{1,0:T(8,128)(2,1)} %wi_ref.1, f32[1,1024]{1,0:T(1,128)} %bitcast.11, ...), custom_call_target="tpu_custom_call" | custom-call | tf_op jit(solution)/shard_map/mixer/pallas_call | solution.py:526
  81.0 0.0 copy-start
  81.0 1.9 %copy.14 = bf16[1,128,2048]{2,1,0:T(8,128)(2,1)} copy(bf16[1,128,2048]{2,1,0:T(8,128)(2,1)} %bitcast.9) | data formatting | bytes 1048576
  82.9 0.0 copy-done
  82.9 0.6 copy.15
Async XLA Ops:
  81.0 1.9 %copy-start = (f32[1,512]{1,0:T(1,128)S(1)}, f32[1,512]{1,0:T(1,128)}, u32[]{:S(2)}) copy-start(f32[1,512]{1,0:T(1,128)} %get-tuple-element.9) | copy-start | bytes 6148

commit v3 on v2

--- a/solution.py
+++ b/solution.py
@@ -10,7 +10,6 @@
 BLOCK = 64
 EPSILON = 1e-05
 PIECES = 4
-LAG = 2
 LOG_ROWS = 8
 MESH = pl.DeviceIdType.MESH
 BF = jnp.bfloat16
@@ -44,11 +43,11 @@
     def kernel(
         tok_ref, gain_ref, wq_ref, wf_ref, wi_ref, gap_ref, ext_ref, init_ref, hgain_ref, wout_ref,
         mixed_ref, final_ref,
-        tok_in, init_in, tokens, weights, others, w_out, ext_all, pad, raw, keys, cums, entering,
-        offsets, local_out, q_glob, own_state, states, gated, gated_in, final_buf, final_in, prefix,
+        tok_in, gain_in, gain_rows, gap_in, hgain_in, init_in, tokens, weights, others, w_out, ext_all, pad, pick, early, raw, keys, cums, entering,
+        offsets, local_out, q_glob, own_state, pair_in, pair_state, states, gated, gated_in, final_buf, final_in, prefix,
         load_sem, tok_send, tok_recv, wo_send, wo_recv, z_send, z_recv, zo_send, zo_recv,
         d_send, d_recv, do_send, do_recv, ext_send, ext_recv,
-        st_send, st_recv, g_send, g_recv, f_send, f_recv,
+        pair_send, pair_recv, st_send, st_recv, g_send, g_recv, f_send, f_recv,
     ):
         s = lax.axis_index("sp")
         t = lax.axis_index("tp")
@@ -92,20 +91,23 @@
             )
         pl.semaphore_signal(barrier, inc=1, device_id=at_sp(behind), device_id_type=MESH)
 
-        def source_at(step):
-            return (s + n_sp - step + 2 * core * step) % n_sp
-
-        def source_beside(step):
-            return (s + n_sp + step - 2 * core * step) % n_sp
+        def source_of(slot):
+            step = (slot + 1) // 2
+            return (s + n_sp - step) % n_sp if slot % 2 else (s + step) % n_sp
 
         def slot_at(step):
             if step == 0:
                 return 0
             return n_sp - 1 if step == half else 2 * step - 1 + core
 
-        def w_piece(ref, source, m):
-            rows = pl.ds(pl.multiple_of(source * k_rows, k_rows), k_rows)
-            return ref.at[rows, pl.ds(m * width_own, width_own)]
+        def slot_beside(step):
+            return n_sp - 1 if step == half else 2 * step - core
+
+        def w_piece(ref, slot, m):
+            start = slot * k_rows
+            if not isinstance(start, int):
+                start = pl.multiple_of(start, k_rows)
+            return ref.at[pl.ds(start, k_rows), pl.ds(m * width_own, width_own)]
 
         def own_channels(index):
             return pl.ds(pl.multiple_of(index * width_own, width_own), width_own)
@@ -118,26 +120,39 @@
             loads.append(copy)
 
         load(tok_ref, tok_in)
+        load(gain_ref, gain_in)
         for m, ref in enumerate((wq_ref, wf_ref, wi_ref)):
-            load(ref.at[:, lanes_partner], w_piece(others, s, m))
-            load(ref.at[:, lanes], w_piece(weights, s, m))
+            load(ref.at[:, lanes_partner], w_piece(others, 0, m))
+            load(ref.at[:, lanes], w_piece(weights, 0, m))
         load(ext_ref, ext_all.at[t])
         load(wout_ref.at[own_channels(t), :], w_out.at[t, 0])
         load(wout_ref.at[own_channels(partner), :], w_out.at[partner, 0])
         load(init_ref.at[own_channels(t), :], init_in)
+        load(gap_ref, gap_in)
+        load(hgain_ref, hgain_in)
 
         loads[0].wait()
-        gain = gain_ref[...].astype(F32).reshape(1, d_model)
+        loads[1].wait()
+        gain = gain_in[...].astype(F32).reshape(1, d_model)
+        gain_rows[...] = gain
         for p in range(PIECES):
             here = slice(p * piece_rows, (p + 1) * piece_rows)
             values = tok_in[here, :].astype(F32)
-            center = values - jnp.mean(values, axis=-1, keepdims=True)
-            spread = jnp.mean(center * center, axis=-1, keepdims=True)
-            normed = center * lax.rsqrt(spread + EPSILON) * gain
-            tokens[pl.ds(pl.multiple_of(t * span + p * piece_rows, piece_rows), piece_rows), :] = (
-                normed.astype(BF)
-            )
-        for copy in loads[1:]:
+            mean = jnp.mean(values, axis=-1, keepdims=True)
+            center = values - mean
+            scale = lax.rsqrt(jnp.mean(center * center, axis=-1, keepdims=True) + EPSILON)
+            there = pl.ds(pl.multiple_of(t * span + p * piece_rows, piece_rows), piece_rows)
+            for slot in range(n_sp):
+                cols = pl.ds(pl.multiple_of(source_of(slot) * k_rows, k_rows), k_rows)
+                normed = (tok_in[here, cols].astype(F32) - mean) * scale * gain_rows[:, cols]
+                tokens[there, slot * k_rows : (slot + 1) * k_rows] = normed.astype(BF)
+        pick_row = lax.broadcasted_iota(jnp.int32, (n_tp * HEADS, n_tp * width_own), 0)
+        pick_col = lax.broadcasted_iota(jnp.int32, (n_tp * HEADS, n_tp * width_own), 1)
+        picked = (pick_col // width_own) * HEADS + (
+            t * (width_own // HEAD) + (pick_col % width_own) // HEAD
+        )
+        pick[...] = jnp.where(pick_row == picked, 1.0, 0.0).astype(BF)
+        for copy in loads[2:]:
             copy.wait()
 
         pl.semaphore_wait(barrier, n_tp - 1 + 1)
@@ -147,23 +162,27 @@
 
         def z_push(step, m, part):
             ref = others if part else weights
-            piece = w_piece(ref, source_at(step - 1), m)
             send(
-                piece, piece, z_send.at[step - 1, m, part], z_recv.at[step - 1, m, part],
-                at_sp(onto),
+                w_piece(ref, slot_at(step - 1), m), w_piece(ref, slot_at(step), m),
+                z_send.at[step - 1, m, part], z_recv.at[step - 1, m, part], at_sp(onto),
             )
 
         def z_step(step):
             for m, part in z_items(step):
-                piece = w_piece(others if part else weights, source_at(step), m)
+                piece = w_piece(others if part else weights, slot_at(step), m)
                 arrived(piece, z_recv.at[step - 1, m, part])
                 if step < half and (m, part) in z_items(step + 1):
                     z_push(step + 1, m, part)
                 if part:
                     send(
-                        piece, w_piece(weights, source_at(step), m), d_send.at[step - 1, m],
+                        piece, w_piece(weights, slot_at(step), m), d_send.at[step - 1, m],
                         d_recv.at[step - 1, m], at_tp(partner),
                     )
+
+        def z_beside(step):
+            for m, part in z_items(step):
+                if part:
+                    arrived(w_piece(weights, slot_beside(step), m), d_recv.at[step - 1, m])
 
         def zo_parts(step):
             return (1, 0) if step < half else (0,)
@@ -191,8 +210,7 @@
                 )
 
         def zo_beside(step, part):
-            slot = n_sp - 1 if step == half else 2 * step - core
-            arrived(w_out.at[t if part else partner, slot], do_recv.at[step - 1, part])
+            arrived(w_out.at[t if part else partner, slot_beside(step)], do_recv.at[step - 1, part])
 
         for m, part in z_items(1):
             z_push(1, m, part)
@@ -268,47 +286,79 @@
             if step <= half:
                 zo_step(step)
 
-        taken = 0
-        for step in range(1, half + 1):
-            z_step(step)
-            while taken < 6 and (taken < step or step == half):
-                tok_ring.take(taken)
-                taken += 1
-            if step >= LAG:
-                wo_advance(step - LAG)
-        for step in range(1, half):
-            for m in range(3):
-                arrived(w_piece(weights, source_beside(step), m), d_recv.at[step - 1, m])
-        tok_ring.partners((0, 1, n_chips - 1, 2))
-        for i in range(1, n_tp):
-            arrived(ext_all.at[(t + i) % n_tp], ext_recv.at[(t + i) % n_tp])
-
-        rows_step = 256
-        for r in range(0, rows_all, rows_step):
-            raw[r : r + rows_step, :] = mm(tokens[r : r + rows_step, :], weights[...]).astype(BF)
-
-        wo_advance(half - LAG + 1)
-        gap = gap_ref[:, lanes]
+        reached = [0]
+
+        def wo_go(last):
+            while reached[0] <= last:
+                wo_advance(reached[0])
+                reached[0] += 1
+
+        def project(block, first_slot, last_slot):
+            rows = slice(block * 2 * span, (block + 1) * 2 * span)
+            part = slice(first_slot * k_rows, last_slot * k_rows)
+            early[rows, :] = mm(tokens[rows, part], weights[part, :])
+
+        n_most = n_sp - 3
+
+        wo_go(0)
+
         row_i = lax.broadcasted_iota(jnp.int32, (2 * BLOCK, 2 * BLOCK), 0)
         col_i = lax.broadcasted_iota(jnp.int32, (2 * BLOCK, 2 * BLOCK), 1)
         causal = jnp.logical_and(row_i >= col_i, row_i // BLOCK == col_i // BLOCK)
         tri = jnp.where(causal, 1.0, 0.0).astype(BF)
         tri3 = jnp.concatenate([tri, tri, tri], axis=1)
-        head_row = lax.broadcasted_iota(jnp.int32, (HEADS, width_own), 0)
-        head_col = lax.broadcasted_iota(jnp.int32, (HEADS, width_own), 1)
-        pick = jnp.where(
-            head_row == t * (width_own // HEAD) + head_col // HEAD, 1.0, 0.0
-        ).astype(BF)
-        pick3 = jnp.concatenate([pick, pick, pick], axis=0)
+        def extra_sums():
+            values = ext_all[...].reshape(n_tp * HEADS, span)
+            sums = mm(jnp.concatenate(split3(values), axis=1), tri3, NT)
+            sums = split3(sums.T)
+            for i in range(n_tp):
+                chosen = pick[:, i * width_own : (i + 1) * width_own]
+                cums[i * span : (i + 1) * span, :] = mm(
+                    jnp.concatenate(sums, axis=1), jnp.concatenate([chosen] * 3, axis=0)
+                )
+
+        taken = 0
+        for step in range(1, half):
+            z_step(step)
+            wo_go(step)
+            while taken < 6 and (taken < step or step == half - 1):
+                tok_ring.take(taken)
+                taken += 1
+        tok_ring.partners((0, 1, n_chips - 1, 2))
+        for step in range(1, half - 1):
+            z_beside(step)
+        for i in range(1, n_tp):
+            arrived(ext_all.at[(t + i) % n_tp], ext_recv.at[(t + i) % n_tp])
+        extra_sums()
+        for block in range(n_chips):
+            project(block, 0, n_most)
+        z_step(half)
+        z_beside(half - 1)
+        wo_go(half)
+        rest = slice(n_most * k_rows, n_sp * k_rows)
+        rows_step = 256
+        for r in range(0, rows_all, rows_step):
+            rows = slice(r, r + rows_step)
+            raw[rows, :] = (early[rows, :] + mm(tokens[rows, rest], weights[rest, :])).astype(BF)
+
+        gaps = gap_in[...].reshape(1, n_tp * width_own)
+        gains = hgain_in[...].astype(F32).reshape(1, n_tp * width_own)
+        gap, head_gain = gaps[:, :width_own], gains[:, :width_own]
+        for i in range(1, n_tp):
+            cols = slice(i * width_own, (i + 1) * width_own)
+            gap = jnp.where(t == i, gaps[:, cols], gap)
+            head_gain = jnp.where(t == i, gains[:, cols], head_gain)
         for i in range(n_tp):
             here = slice(i * span, (i + 1) * span)
             forget = raw[here, width_own : 2 * width_own].astype(F32)
             key = gap / (1.0 + jnp.exp(forget))
-            extra = mm(jnp.concatenate(split3(ext_all[i]), axis=0), pick3, TN)
-            log_keep = jnp.log1p(-key) + extra
-            cums[here, :] = mm(tri3, jnp.concatenate(split3(log_keep), axis=0))
+            kept = mm(tri3, jnp.concatenate(split3(jnp.log1p(-key)), axis=0))
+            cums[here, :] = cums[here, :] + kept
             keys[here, :] = key
 
+        wo_go(half + 1)
+        wo_ring.take(0)
+        wo_ring.take(1)
         lane = lax.broadcasted_iota(jnp.int32, (HEAD, width_own), 1)
         first = lane < HEAD
         state = jnp.zeros((HEAD, width_own), F32)
@@ -322,30 +372,49 @@
             offsets[b] = offset
             state = state * jnp.exp(total) + jnp.where(first, added[:HEAD], added[HEAD:])
             offset = offset + total
-        own_state[:HEAD] = state.astype(BF)
-        o_high, o_middle, o_low = split3(offset)
         log_row = lax.broadcasted_iota(jnp.int32, (LOG_ROWS, width_own), 0)
-        own_state[HEAD:] = jnp.where(
-            log_row == 0, o_high.astype(F32),
-            jnp.where(log_row == 1, o_middle.astype(F32),
-                      jnp.where(log_row == 2, o_low.astype(F32), 0.0)),
-        ).astype(BF)
+
+        def pack(ref, value, logs):
+            ref[:HEAD] = value.astype(BF)
+            high, middle, low = split3(logs)
+            ref[HEAD:] = jnp.where(
+                log_row == 0, high.astype(F32),
+                jnp.where(log_row == 1, middle.astype(F32),
+                          jnp.where(log_row == 2, low.astype(F32), 0.0)),
+            ).astype(BF)
+
+        def unpack(ref):
+            logs = ref[HEAD:].astype(F32)
+            return ref[:HEAD].astype(F32), logs[0:1] + logs[1:2] + logs[2:3]
+
+        pair_copy = pltpu.make_async_remote_copy(
+            src_ref=own_state, dst_ref=pair_in, send_sem=pair_send, recv_sem=pair_recv,
+            device_id=at_sp((s + 1) % n_sp), device_id_type=MESH,
+        )
 
         def state_copy(j):
             return pltpu.make_async_remote_copy(
-                src_ref=own_state, dst_ref=states.at[s], send_sem=st_send.at[j],
-                recv_sem=st_recv.at[s], device_id=at_sp(j), device_id_type=MESH,
+                src_ref=pair_state, dst_ref=states.at[s // 2], send_sem=st_send.at[j],
+                recv_sem=st_recv.at[s // 2], device_id=at_sp(j), device_id_type=MESH,
             )
 
         def state_push(k, carry):
             state_copy(n_sp - 1 - k).start()
             return carry
 
-        lax.fori_loop(0, n_sp - 1 - s, state_push, 0)
-        for step in range(half - LAG + 2, half + 2):
-            wo_advance(step)
-        for j in range(2):
-            wo_ring.take(j)
+        @pl.when(s % 2 == 0)
+        def _():
+            pack(own_state, state, offset)
+            pair_copy.start()
+
+        @pl.when(s % 2 == 1)
+        def _():
+            pair_copy.wait_recv()
+            value, logs = unpack(pair_in)
+            pack(pair_state, value * jnp.exp(offset) + state, logs + offset)
+            lax.fori_loop(0, n_sp - 1 - s, state_push, 0)
+
+        wo_ring.take(2)
         lane2 = lax.broadcasted_iota(jnp.int32, (span, width_own), 1)
         first2 = lane2 < HEAD
 
@@ -377,8 +446,8 @@
                 local_out[rows, :] = within[part] + seen
                 q_glob[rows, :] = (q_part * jnp.exp(offsets[b])).astype(BF)
 
-        wo_ring.take(2)
         wo_ring.take(3)
+        wo_ring.take(4)
 
         pad[...] = jnp.zeros_like(pad)
         pad[:, :HEAD] = init_in[...]
@@ -386,39 +455,50 @@
 
         def advance(j, value):
             arrived(states.at[j], st_recv.at[j])
-            logs = states[j, HEAD:].astype(F32)
-            total = logs[0:1] + logs[1:2] + logs[2:3]
-            return value * jnp.exp(total) + states[j, :HEAD].astype(F32)
-
-        carried = lax.fori_loop(0, s, advance, carried)
+            added, logs = unpack(states.at[j])
+            return value * jnp.exp(logs) + added
+
+        def advance_one(j, value):
+            added, logs = unpack(pair_in)
+            return value * jnp.exp(logs) + added
+
+        carried = lax.fori_loop(0, s // 2, advance, carried)
+        carried = lax.fori_loop(0, s % 2, advance_one, carried)
         prefix[...] = spread_heads(carried, first).astype(BF)
 
         ones_row = lax.broadcasted_iota(jnp.int32, (width_own, width_own), 0)
         ones_col = lax.broadcasted_iota(jnp.int32, (width_own, width_own), 1)
         same = jnp.where(ones_row // HEAD == ones_col // HEAD, 1.0 / HEAD, 0.0).astype(BF)
         same2 = jnp.concatenate([same, same], axis=0)
-        gains = hgain_ref[...].astype(F32).reshape(1, n_tp * width_own)
-        head_gain = gains[:, :width_own]
-        for i in range(1, n_tp):
-            head_gain = jnp.where(t == i, gains[:, i * width_own : (i + 1) * width_own], head_gain)
-        for i in range(1, n_tp + 1):
-            block = (t + i) % n_tp
-            rows = pl.ds(pl.multiple_of(block * span, span), span)
-            recurrent = local_out[rows, :] + mm(q_glob[rows, :], prefix[...], NT)
-            square = recurrent * recurrent
-            high = square.astype(BF)
-            low = (square - high.astype(F32)).astype(BF)
-            power = mm(jnp.concatenate([high, low], axis=1), same2)
-            done = (recurrent * lax.rsqrt(power + EPSILON) * head_gain).astype(BF)
-            if i < n_tp:
-                gated[rows, :] = done
+        targets = [
+            ((chip + where) % n_chips) * 2 + side
+            for where in (2, 1, n_chips - 1, 0) for side in (core, 1 - core)
+        ]
+        targets = targets[:6] + [partner, t]
+
+        def gate(group, first_count):
+            for block in group:
+                rows = pl.ds(pl.multiple_of(block * span, span), span)
+                recurrent = local_out[rows, :] + mm(q_glob[rows, :], prefix[...], NT)
+                square = recurrent * recurrent
+                high = square.astype(BF)
+                low = (square - high.astype(F32)).astype(BF)
+                power = mm(jnp.concatenate([high, low], axis=1), same2)
+                done = (recurrent * lax.rsqrt(power + EPSILON) * head_gain).astype(BF)
+                if block is t:
+                    gated_in[:, lanes] = done
+                else:
+                    gated[rows, :] = done
+            for count, block in enumerate(group, first_count):
+                if block is t:
+                    continue
+                rows = pl.ds(pl.multiple_of(block * span, span), span)
                 send(
-                    gated.at[rows, :], gated_in.at[:, lanes], g_send.at[i], g_recv.at[t],
-                    at_tp(block),
+                    gated.at[rows, :], gated_in.at[:, lanes], g_send.at[count],
+                    g_recv.at[t], at_tp(block),
                 )
-            else:
-                gated_in[:, lanes] = done
-
+
+        gate(targets[:4], 0)
         part_rows = HEAD // n_tp
 
         def final_copies(act):
@@ -450,7 +530,7 @@
                 final_buf[...] = jnp.concatenate([last, last], axis=0).T
                 final_copies("start")
 
-        wo_ring.take(4)
+        gate(targets[4:], 4)
         wo_ring.take(5)
         wo_ring.partners((1, n_chips - 1, 2))
         for step in range(1, half + 1):
@@ -464,10 +544,6 @@
                 g_recv.at[other],
             )
 
-        def source_of(slot):
-            step = (slot + 1) // 2
-            return (s + n_sp - step) % n_sp if slot % 2 else (s + step) % n_sp
-
         for pair in range(n_sp // 2):
             right_side = jnp.concatenate(
                 [w_out[:, slot].reshape(n_tp * width_own, -1) for slot in (2 * pair, 2 * pair + 1)],
@@ -499,7 +575,12 @@
             state_copy(n_sp - 1 - k).wait_send()
             return carry
 
-        lax.fori_loop(0, n_sp - 1 - s, state_end, 0)
+        pl.when(s % 2 == 0)(pair_copy.wait_send)
+
+        @pl.when(s % 2 == 1)
+        def _():
+            lax.fori_loop(0, n_sp - 1 - s, state_end, 0)
+
         for copy in sent:
             copy.wait_send()
 
@@ -520,19 +601,23 @@
         blocks = rows // BLOCK
         flat = HEADS * HEAD * HEAD // (n_sp * n_tp)
         vmem = pl.BlockSpec(memory_space=pltpu.VMEM)
-        hbm = pl.BlockSpec(memory_space=pl.ANY)
+        hbm = pl.BlockSpec(memory_space=pltpu.HBM)
         half = n_sp // 2
         dma = pltpu.SemaphoreType.DMA
         mixed, final_state = pl.pallas_call(
             make_kernel(n_sp, n_tp, span, own, d_model),
             out_shape=(
-                jax.ShapeDtypeStruct((span, d_model), BF),
-                jax.ShapeDtypeStruct((1, flat), F32),
+                pltpu.VMEM((span, d_model), BF),
+                pltpu.VMEM((1, flat), F32),
             ),
-            in_specs=[hbm, vmem, hbm, hbm, hbm, vmem, hbm, hbm, vmem, hbm],
+            in_specs=[hbm] * 10,
             out_specs=(vmem, vmem),
             scratch_shapes=[
                 pltpu.VMEM((span, d_model), BF),
+                pltpu.VMEM((d_model,), BF),
+                pltpu.VMEM((1, d_model), F32),
+                pltpu.VMEM((width,), F32),
+                pltpu.VMEM((width,), BF),
                 pltpu.VMEM((own, HEAD), F32),
                 pltpu.VMEM((rows, d_model), BF),
                 pltpu.VMEM((d_model, 3 * own), BF),
@@ -540,6 +625,8 @@
                 pltpu.VMEM((n_tp, n_sp, own, d_model // n_sp), BF),
                 pltpu.VMEM((n_tp, HEADS, span), F32),
                 pltpu.VMEM((span, own), F32),
+                pltpu.VMEM((n_tp * HEADS, n_tp * own), BF),
+                pltpu.VMEM((rows, 3 * own), F32),
                 pltpu.VMEM((rows, 3 * own), BF),
                 pltpu.VMEM((rows, own), F32),
                 pltpu.VMEM((rows, own), F32),
@@ -548,18 +635,20 @@
                 pltpu.VMEM((rows, own), F32),
                 pltpu.VMEM((rows, own), BF),
                 pltpu.VMEM((HEAD + LOG_ROWS, own), BF),
-                pltpu.VMEM((n_sp, HEAD + LOG_ROWS, own), BF),
+                pltpu.VMEM((HEAD + LOG_ROWS, own), BF),
+                pltpu.VMEM((HEAD + LOG_ROWS, own), BF),
+                pltpu.VMEM((n_sp // 2, HEAD + LOG_ROWS, own), BF),
                 pltpu.VMEM((rows, own), BF),
                 pltpu.VMEM((span, width), BF),
                 pltpu.VMEM((own, 2 * HEAD), F32),
                 pltpu.VMEM((HEAD // n_tp, 2 * HEAD), F32),
                 pltpu.VMEM((own, own), BF),
-                dma((11,)),
+                dma((14,)),
                 dma((28,)), dma((n_tp, PIECES)), dma((28,)), dma((n_tp, PIECES)),
                 dma((half, 3, 2)), dma((half, 3, 2)), dma((half, 2)), dma((half, 2)),
                 dma((half, 3)), dma((half, 3)), dma((half, 2)), dma((half, 2)),
                 dma((n_tp,)), dma((n_tp,)),
-                dma((n_sp,)), dma((n_sp,)),
+                dma, dma, dma((n_sp,)), dma((n_sp // 2,)),
                 dma((n_tp,)), dma((n_tp,)),
                 dma((HEADS // n_tp, n_tp)), dma,
             ],
@@ -571,7 +660,7 @@
             tokens.reshape(span, d_model),
             norm_gain,
             w_query, w_forget, w_input,
-            floor_gap.reshape(1, width),
+            floor_gap,
             jnp.swapaxes(extra_decay, 1, 2).reshape(HEADS, span),
             init_state.reshape(HEADS * HEAD, HEAD),
             head_norm_gain,

time: 83.7 us -> 74.1 us (0.89)
  Pallas kernels: 80.4 us -> 72 us
  local copies, waits for them, and re-layouts: 2.46 us -> 1.37 us
    pallas_call x1, Pallas kernels: 80.4 us -> 72 us  [body(): pl.pallas_call(make_kernel(n_sp, n_tp, span, own, d_model), out_shape=(pl...]
    unnamed x4 -> x2, local copies, waits for them, and re-layouts: 2.46 us -> 1.37 us
where the time goes in v3:
time: 74.1 us; the launch traced here: 74 us
  Pallas kernels  72 us (97%)
  local copies, waits for them, and re-layouts  1.37 us (2%)
    pallas_call x1, Pallas kernels, body(): pl.pallas_call(make_kernel(n_sp, n_tp, span, own, d_model), out_shape=(pl...  72 us

profile of v3, /device:TPU:33, one launch (start us, length us, event | category | flops | bytes accessed | tf_op | source)
XLA Modules:
  0.0 74.0 jit_solution(5872356958021148586)
XLA Ops:
  0.6 72.0 %mixer.1 = (bf16[128,2048]{1,0:T(8,128)(2,1)S(1)}, f32[1,512]{1,0:T(1,128)S(1)}) custom-call(bf16[128,2048]{1,0:T(8,128)(2,1)} %bitcast.7, bf16[2048]{0:T(1024)(128)(2,1)} %gain_ref.1, bf16[128,1024]{1,0:T(8,128)(2,1)} %wq_ref.1, bf16[128,1024]{1,0:T(8,128)(2,1)} %wf_ref.1, bf16[128,1024]{1,0:T(8,128)(2,1)} %wi_ref.1, f32[1024]{0:T(1024)} %gap_ref.1, ...), custom_call_target="tpu_custom_call" | custom-call | tf_op jit(solution)/shard_map/mixer/pallas_call | solution.py:607
  72.6 0.8 %copy.14 = bf16[1,128,2048]{2,1,0:T(8,128)(2,1)} copy(bf16[1,128,2048]{2,1,0:T(8,128)(2,1)S(1)} %bitcast.6) | data formatting | bytes 1048576
  73.4 0.6 copy.15
